TPU v7x, 256 devices: a whole 4x4x8 slice. The times are simulated.
256 devices in a mesh: sp: 16 (over y, x), tp: 16 (over z, core).
Axes of the slice: x: 4, y: 4, z: 8, core: 2. Of those that a mesh axis runs over, the one named last changes fastest.
Arguments:
- conv_value: bfloat16 [49152, 2048], P('sp', 'tp'), may hold values from -48 to 48
- conv_gate: bfloat16 [49152, 2048], P('sp', 'tp'), may hold values from -6 to 6
- doc_ids: int32 [49152], P('sp'), may hold values from 0 to 15, never falling along the last dimension, each value on 1 to 9216 neighbouring positions
- conv_kernel: bfloat16 [31, 2048], P(None, 'tp'), may hold values from -1 to 1
- norm_gain_conv: float32 [2048], replicated, may hold values from 0.1 to 1.9
- norm_bias_conv: float32 [2048], replicated, may hold values from -3 to 3
- proj_weight: bfloat16 [2048, 2048], P('tp'), may hold values from -0.125 to 0.125
- residual: bfloat16 [49152, 2048], P(('sp', 'tp')), may hold values from -6 to 6
- norm_gain_moe: float32 [2048], replicated, may hold values from 0.1 to 1.9
- group_router: bfloat16 [2048, 2], replicated, may hold values from -0.125 to 0.125
- expert_router: bfloat16 [2048, 16], replicated, may hold values from -0.125 to 0.125
- routing: int32 [49152, 2], P(('sp', 'tp')), may hold values from 0 to 15, as said below
- expert_gate_w: bfloat16 [16, 2048, 512], P('sp'), may hold values from -0.125 to 0.125
- expert_up_w: bfloat16 [16, 2048, 512], P('sp'), may hold values from -0.125 to 0.125
- expert_down_w: bfloat16 [16, 512, 2048], P('sp'), may hold values from -0.25 to 0.25
Outputs:
- output: bfloat16 [49152, 2048], P(('sp', 'tp'))
Inputs may be any that keep to these rules, and one draw needn't show every extreme that they name: `routing`: both numbers of a row are different experts of one group (expert // 8); within the rows of one device (aligned blocks of 192 rows) every expert is named exactly 24 times.
All inputs are finite; a program needn't handle non-finite values.
Results may differ from a plain program's by a relative error of at most 0.015.
Values may be sent and summed in bfloat16 or wider, within the bound.
No kernel may reach another device: no remote copies, remote signals or barrier semaphores. Data moves between devices by JAX's collectives and lax.ppermute only.
A program may use at most 64 MiB of HBM per device.

v0:
```python
import functools

import jax
import jax.numpy as jnp
from jax import lax
from jax.experimental import pallas as pl
from jax.experimental.pallas import tpu as pltpu
from jax.sharding import PartitionSpec as P


epsilon = 1e-06
CHUNK = 64
ORDER = (0, 4, 2, 6, 1, 5, 3, 7)
NEAR = (0, 1, 3, 2)
VMEM = pl.BlockSpec(memory_space=pltpu.VMEM)
SMEM = pl.BlockSpec(memory_space=pltpu.SMEM)


def params(mib):
    return pltpu.CompilerParams(vmem_limit_bytes=mib * 1024 * 1024)


def conv_kernel_body(
    place_ref,
    starts_ref,
    edge_ref,
    value_ref,
    gate_ref,
    value_halo_ref,
    gate_halo_ref,
    rim_ref,
    kernel_ref,
    *refs,
):
    outs, (taps, rows, masked, total) = refs[:-4], refs[-4:]
    step = pl.program_id(0)
    at_tile = step ^ place_ref[0]
    tile, lanes = value_ref.shape
    tap_count = kernel_ref.shape[0]

    def gated(value, gate):
        return (
            (value[...].astype(jnp.float32) * jax.nn.sigmoid(gate[...].astype(jnp.float32)))
            .astype(jnp.bfloat16)
            .astype(jnp.float32)
        )

    @pl.when(step == 0)
    def _():
        kernel = kernel_ref[...].astype(jnp.float32)
        for tap in range(tap_count):
            taps[8 * tap : 8 * tap + 8, :] = jnp.broadcast_to(kernel[tap : tap + 1, :], (8, lanes))

    @pl.when(at_tile == 0)
    def _():
        rows[0:32, :] = rim_ref[...].astype(jnp.float32)

    @pl.when(at_tile > 0)
    def _():
        rows[0:32, :] = gated(value_halo_ref, gate_halo_ref)

    rows[32:, :] = gated(value_ref, gate_ref)

    def convolve(source, at):
        acc = jnp.zeros((CHUNK // 8, 8, lanes), jnp.float32)
        for tap in range(tap_count):
            window = source[at + 2 + tap : at + 2 + tap + CHUNK, :].reshape(CHUNK // 8, 8, lanes)
            acc = acc + window * taps[8 * tap : 8 * tap + 8, :][None]
        return acc.reshape(CHUNK, lanes)

    base = at_tile * tile
    low, high = edge_ref[0, at_tile], edge_ref[1, at_tile]
    whole = jnp.logical_and(low == high, starts_ref[low] <= base)

    @pl.when(whole)
    def _():
        for at in range(0, tile, CHUNK):
            total[at : at + CHUNK, :] = convolve(rows, at)

    @pl.when(jnp.logical_not(whole))
    def _():
        total[...] = jnp.zeros_like(total)

        def one_document(doc, carry):
            first = starts_ref[doc] - base + 2
            last = starts_ref[doc + 1] - base + 2
            position = lax.broadcasted_iota(jnp.int32, rows.shape, 0)
            masked[...] = jnp.where(
                jnp.logical_and(position >= first, position < last), rows[...], jnp.float32(0.0)
            )
            for at in range(0, tile, CHUNK):
                place = lax.broadcasted_iota(jnp.int32, (CHUNK, lanes), 0) + (at + 32)
                inside = jnp.logical_and(place >= first, place < last)
                total[at : at + CHUNK, :] += jnp.where(
                    inside, convolve(masked, at), jnp.float32(0.0)
                )
            return carry

        lax.fori_loop(low, high + 1, one_document, 0)

    for slot, out in enumerate(outs):

        @pl.when(step == slot)
        def _(out=out):
            out[...] = total[...].astype(out.dtype)


def convolve_tokens(place, starts, edges, value, gate, rim, kernel, parts):
    tokens, lanes = value.shape
    taps = kernel.shape[0]
    tile = tokens // parts

    def here(i, place, *_):
        return (i ^ place[0], 0)

    def halo(i, place, *_):
        return (jnp.maximum((i ^ place[0]) * (tile // 32) - 1, 0), 0)

    def whole(i, *_):
        return (0, 0)

    return pl.pallas_call(
        conv_kernel_body,
        grid_spec=pltpu.PrefetchScalarGridSpec(
            num_scalar_prefetch=3,
            grid=(parts,),
            in_specs=[
                pl.BlockSpec((tile, lanes), here),
                pl.BlockSpec((tile, lanes), here),
                pl.BlockSpec((32, lanes), halo),
                pl.BlockSpec((32, lanes), halo),
                pl.BlockSpec((32, lanes), whole),
                pl.BlockSpec((taps, lanes), whole),
            ],
            out_specs=[pl.BlockSpec((tile, lanes), whole)] * parts,
            scratch_shapes=[
                pltpu.VMEM((8 * taps, lanes), jnp.float32),
                pltpu.VMEM((tile + 32, lanes), jnp.float32),
                pltpu.VMEM((tile + 32, lanes), jnp.float32),
                pltpu.VMEM((tile, lanes), jnp.float32),
            ],
        ),
        out_shape=[jax.ShapeDtypeStruct((tile, lanes), jnp.bfloat16)] * parts,
        compiler_params=params(12),
        name="gated_conv",
    )(place, starts, edges, value, gate, value, gate, rim, kernel)


def rim_body(value_ref, gate_ref, ids_ref, out_ref):
    tokens, lanes = value_ref.shape
    tail = slice(tokens - 32, tokens)
    out_ref[0:32, :] = (
        value_ref[tail, :].astype(jnp.float32)
        * jax.nn.sigmoid(gate_ref[tail, :].astype(jnp.float32))
    ).astype(jnp.bfloat16)
    row = lax.broadcasted_iota(jnp.int32, (32, lanes), 0)
    ids = jnp.zeros((32, lanes), jnp.int32)
    for place in range(32):
        ids = jnp.where(row == place, ids_ref[tokens - 32 + place], ids)
    out_ref[32:64, :] = ids.astype(jnp.float32).astype(jnp.bfloat16)


def slots_body(capacity, place_ref, routing_ref, spread_ref, first_ref, second_ref, choice_ref):
    count = routing_ref.shape[1]
    slots = spread_ref.shape[0]
    row = lax.broadcasted_iota(jnp.int32, (count, count), 0)
    column = lax.broadcasted_iota(jnp.int32, (count, count), 1)
    role, device = place_ref[5], place_ref[4]

    def ones(mask):
        return jnp.where(mask, jnp.float32(1.0), jnp.float32(0.0))

    def slot_of(expert, position):
        apart = expert ^ device
        swapped = (apart & 3) * 4 + (apart >> 2)
        return jnp.where(role == 0, swapped, apart) * capacity + position.astype(jnp.int32)

    sub = lax.broadcasted_iota(jnp.int32, (16, count), 0)
    one, two = routing_ref[0:1, :], routing_ref[1:2, :]
    named = jnp.logical_or(sub == one, sub == two)
    before = jnp.dot(
        ones(named).astype(jnp.bfloat16),
        ones(row < column).astype(jnp.bfloat16),
        preferred_element_type=jnp.float32,
    )
    slot = lax.broadcasted_iota(jnp.int32, (slots, count), 0)
    targets = []
    for chosen in (one, two):
        position = jnp.sum(jnp.where(sub == chosen, before, 0.0), axis=0, keepdims=True)
        targets.append(slot_of(chosen, position))
    spread_ref[...] = ones(jnp.logical_or(slot == targets[0], slot == targets[1])).astype(
        jnp.bfloat16
    )

    def upright(line):
        turned = jnp.sum(
            jnp.where(row == column, line.astype(jnp.float32), 0.0), axis=1, keepdims=True
        )
        return turned.astype(jnp.int32)

    slot = lax.broadcasted_iota(jnp.int32, (count, slots), 1)
    for target, out in zip(targets, (first_ref, second_ref), strict=True):
        out[...] = ones(slot == upright(target)).astype(jnp.bfloat16)
    lane = lax.broadcasted_iota(jnp.int32, choice_ref.shape, 1)
    choice_ref[...] = jnp.where(lane == 0, upright(one), upright(two))


def stats_body(*refs):
    raw_refs, out_ref = refs[:-1], refs[-1]
    count, lanes = raw_refs[0].shape
    summed = jnp.zeros((count, lanes), jnp.float32)
    for raw in raw_refs:
        summed = summed + raw[...].astype(jnp.float32)
    average = jnp.sum(summed, axis=1, keepdims=True) * jnp.float32(1.0 / (lanes * len(raw_refs)))
    squares = jnp.zeros((count, lanes), jnp.float32)
    for raw in raw_refs:
        centered = raw[...].astype(jnp.float32) - average
        squares = squares + centered * centered
    squares = jnp.sum(squares, axis=1, keepdims=True)
    lane = lax.broadcasted_iota(jnp.int32, (count, lanes), 1)
    out_ref[...] = jnp.where(lane == 0, average, squares)


def activate_body(order, place_ref, mine_ref, other_ref, gain_ref, bias_ref, *refs):
    raw_refs, out_ref = refs[:-1], refs[-1]
    rows, lanes = raw_refs[0].shape
    count = rows // 2
    half = lanes * len(raw_refs)
    core = place_ref[1]
    for block in range(2):
        at = pl.ds(pl.multiple_of((core ^ block) * count, count), count)
        to = slice(block * count, block * count + count)
        mine, other = mine_ref[at, :], other_ref[at, :]
        average = (mine[:, 0:1] + other[:, 0:1]) * jnp.float32(0.5)
        apart = mine[:, 0:1] - other[:, 0:1]
        spread = mine[:, 1:2] + other[:, 1:2] + apart * apart * jnp.float32(half / 2)
        scale = lax.rsqrt(spread * jnp.float32(0.5 / half) + epsilon)
        for slot, raw in enumerate(raw_refs):
            part = 2 * (place_ref[0] ^ order[slot]) + core
            value = (raw[at, :].astype(jnp.float32) - average) * scale * gain_ref[part] + bias_ref[
                part
            ]
            out_ref[to, slot * lanes : slot * lanes + lanes] = jax.nn.silu(value).astype(
                jnp.bfloat16
            )


def partial_body(
    place_ref,
    active_ref,
    low_ref,
    low_1_ref,
    low_32_ref,
    high_ref,
    high_3_ref,
    high_12_ref,
    mine_ref,
    other_ref,
    weight,
    sems,
):
    _, slots, depth, group = weight.shape
    count = mine_ref.shape[0]
    v, u = place_ref[2], place_ref[3]
    sources = (
        (0, low_ref, high_ref),
        (1, low_1_ref, high_12_ref.at[0]),
        (3, low_32_ref.at[0], high_3_ref),
        (2, low_32_ref.at[1], high_12_ref.at[1]),
    )
    copies = []
    for number, (_, *halves) in enumerate(sources):
        for side, half in enumerate(halves):
            for nth, near in enumerate(NEAR):
                copy = pltpu.make_async_copy(
                    half.at[nth],
                    weight.at[
                        number,
                        pl.ds(4 * side, 4),
                        :,
                        pl.ds(pl.multiple_of((u ^ near) * 128, 128), 128),
                    ],
                    sems.at[8 * number + 4 * side + nth],
                )
                copy.start()
                copies.append(copy)
    for number, (far, *_) in enumerate(sources):
        for nth in range(8):
            copies[8 * number + nth].wait()
        product = jnp.dot(
            active_ref[...],
            weight[number].reshape(slots * depth, group),
            preferred_element_type=jnp.float32,
        )
        to = pl.ds(pl.multiple_of((v ^ far) * group, group), group)
        mine_ref[:, to] = product[:count]
        other_ref[:, to] = product[count:].astype(other_ref.dtype)


def state_body(
    groups,
    experts,
    mine_ref,
    other_ref,
    residual_ref,
    gain_moe_ref,
    router_ref,
    choice_ref,
    spread_ref,
    state_ref,
    mix_ref,
    *outgoing_refs,
):
    projected = (
        residual_ref[...].astype(jnp.float32) + mine_ref[...] + other_ref[...].astype(jnp.float32)
    )
    state = projected.astype(jnp.bfloat16)
    state_ref[...] = state
    state = state.astype(jnp.float32)
    power = jnp.mean(state * state, axis=1, keepdims=True)
    normed = (state * lax.rsqrt(power + epsilon) * gain_moe_ref[...]).astype(jnp.bfloat16)
    outgoing = jnp.dot(spread_ref[...], normed, preferred_element_type=jnp.float32)
    block = outgoing_refs[0].shape[0]
    for number, ref in enumerate(outgoing_refs):
        ref[...] = outgoing[number * block : number * block + block].astype(jnp.bfloat16)
    logits = lax.dot_general(
        normed, router_ref[...], (((1,), (1,)), ((), ())), preferred_element_type=jnp.float32
    )
    lane = lax.broadcasted_iota(jnp.int32, logits.shape, 1)
    one, two = choice_ref[:, 0:1], choice_ref[:, 1:2]
    group = one // (experts // groups)

    def pick(mask, array):
        return jnp.sum(jnp.where(mask, array, jnp.float32(0.0)), axis=1, keepdims=True)

    raised = jnp.exp(logits)
    in_groups = jnp.logical_and(lane >= experts, lane < experts + groups)
    group_prob = pick(lane == experts + group, raised) / pick(in_groups, raised)
    first = jnp.exp(pick(lane == one, logits))
    second = jnp.exp(pick(lane == two, logits))
    both = first + second
    mix_ref[...] = jnp.where(
        lane == 0, group_prob * first / both, jnp.where(lane == 1, group_prob * second / both, 0.0)
    )


def experts_body(rows_ref, gate_ref, up_ref, down_ref, out_ref):
    rows = rows_ref[...]
    gate = jnp.dot(rows, gate_ref[...], preferred_element_type=jnp.float32)
    up = jnp.dot(rows, up_ref[...], preferred_element_type=jnp.float32)
    hidden = (jax.nn.silu(gate) * up).astype(jnp.bfloat16)
    out_ref[...] = jnp.dot(hidden, down_ref[...], preferred_element_type=jnp.float32).astype(
        jnp.bfloat16
    )


def mix_body(state_ref, first_ref, second_ref, mix_ref, *refs):
    returned_refs, out_ref = refs[:-1], refs[-1]
    returned = jnp.concatenate([returned[...] for returned in returned_refs], axis=0)
    first = jnp.dot(first_ref[...], returned, preferred_element_type=jnp.float32)
    second = jnp.dot(second_ref[...], returned, preferred_element_type=jnp.float32)
    mixture = mix_ref[:, 0:1] * first + mix_ref[:, 1:2] * second
    out_ref[...] = (state_ref[...].astype(jnp.float32) + mixture).astype(jnp.bfloat16)


def swap(array, dz=0, dc=0):
    flip = dz * 2 + dc
    return lax.ppermute(array, ("sp", "tp"), [(i, i ^ flip) for i in range(256)])


def cross(array, by, turn):
    pairs = [(i, i ^ (by * (16 if (i & 1) == turn else 64))) for i in range(256)]
    return lax.ppermute(array, ("sp", "tp"), pairs)


def role_of(core, y, x):
    return core ^ (x & 1) ^ (y & 1)


def deal(array, by, turn):
    pairs = []
    for i in range(256):
        along_x = role_of(i & 1, i >> 6, i >> 4 & 3) == turn
        pairs.append((i, i ^ (by * (16 if along_x else 64)) ^ (by & 1)))
    return lax.ppermute(array, ("sp", "tp"), pairs)


def shifted(array, axis, by):
    count = lax.axis_size(axis)
    pairs = [(i, i + by) for i in range(count) if 0 <= i + by < count]
    return lax.ppermute(array, axis, pairs)


def body(
    conv_value,
    conv_gate,
    doc_ids,
    conv_kernel,
    norm_gain_conv,
    norm_bias_conv,
    proj_weight,
    residual,
    norm_gain_moe,
    group_router,
    expert_router,
    routing,
    expert_gate_w,
    expert_up_w,
    expert_down_w,
):
    tokens, lanes = conv_value.shape
    rim = conv_kernel.shape[0] - 1
    count, width = residual.shape
    groups, experts = group_router.shape[1], expert_router.shape[1]
    slots = 2 * count
    capacity = slots // experts

    sp, tp = lax.axis_index("sp"), lax.axis_index("tp")
    z, core, y, x = tp >> 1, tp & 1, sp >> 2, sp & 3
    u, v = jnp.where(core == 0, x, y), jnp.where(core == 0, y, x)
    place = jnp.stack([z, core, v, u, sp, role_of(core, y, x)]).astype(jnp.int32)
    depth = proj_weight.shape[0]

    message = pl.pallas_call(
        rim_body,
        in_specs=[VMEM, VMEM, SMEM],
        out_specs=VMEM,
        out_shape=jax.ShapeDtypeStruct((64, lanes), jnp.bfloat16),
        compiler_params=params(8),
        name="tail",
    )(conv_value, conv_gate, doc_ids)
    came = shifted(message, "sp", 1)

    held = lax.dynamic_slice_in_dim(proj_weight, (v * 4 + u) * 128, 128, axis=1)[None]
    for bit in (4, 2, 1):
        other = swap(held, dz=bit)
        held = jnp.concatenate([held, other], axis=0)
    near = [held]
    for d in NEAR[1:]:
        near.append(cross(held, d, 0))
    low, high = (jnp.stack([part[at : at + 4] for part in near]) for at in (0, 4))
    low_1 = cross(low, 1, 1)
    high_3 = cross(high, 3, 1)
    low_32 = cross(jnp.stack([low, low_1]), 3, 1)
    high_12 = cross(jnp.stack([high, high_3]), 1, 1)
    pieces = [low, low_1, low_32, high, high_3, high_12]

    rim_values, rim_ids = came[:32], came[64 - rim :, 0].astype(jnp.int32)
    padded_ids = jnp.concatenate([rim_ids, doc_ids], axis=0)
    bounds = jnp.arange(24, dtype=jnp.int32)
    starts = jnp.sum((padded_ids[None, :] < bounds[:, None]).astype(jnp.int32), axis=1)
    tiles = doc_ids.reshape(8, tokens // 8)
    edges = jnp.stack([tiles[:, 0], tiles[:, -1]])
    convolved = convolve_tokens(
        place, starts, edges, conv_value, conv_gate, rim_values, conv_kernel, 8
    )
    raw = []
    for d in ORDER:
        raw.append(swap(convolved[d], dz=d) if d else convolved[d])

    spread, first_pick, second_pick, choice = pl.pallas_call(
        functools.partial(slots_body, capacity),
        in_specs=[SMEM, VMEM],
        out_specs=[VMEM] * 4,
        out_shape=[
            jax.ShapeDtypeStruct((slots, count), jnp.bfloat16),
            jax.ShapeDtypeStruct((count, slots), jnp.bfloat16),
            jax.ShapeDtypeStruct((count, slots), jnp.bfloat16),
            jax.ShapeDtypeStruct((count, 128), jnp.int32),
        ],
        compiler_params=params(8),
        name="slots",
    )(place, routing.T)
    routers = jnp.concatenate(
        [
            expert_router.T,
            group_router.T,
            jnp.zeros((32 - experts - groups, width), jnp.bfloat16),
        ],
        axis=0,
    )
    rows = 2 * count
    mine = pl.pallas_call(
        stats_body,
        in_specs=[VMEM] * 8,
        out_specs=VMEM,
        out_shape=jax.ShapeDtypeStruct((rows, lanes), jnp.float32),
        compiler_params=params(8),
        name="stats",
    )(*raw)
    other = swap(mine, dc=1)
    active = pl.pallas_call(
        functools.partial(activate_body, ORDER),
        in_specs=[SMEM] + [VMEM] * 12,
        out_specs=VMEM,
        out_shape=jax.ShapeDtypeStruct((rows, 8 * lanes), jnp.bfloat16),
        compiler_params=params(8),
        name="activate",
    )(
        place,
        mine,
        other,
        norm_gain_conv.reshape(-1, 1, lanes),
        norm_bias_conv.reshape(-1, 1, lanes),
        *raw,
    )
    kept, given = pl.pallas_call(
        partial_body,
        in_specs=[SMEM, VMEM] + [pl.BlockSpec(memory_space=pltpu.HBM)] * 6,
        out_specs=[VMEM] * 2,
        out_shape=[
            jax.ShapeDtypeStruct((count, width), jnp.float32),
            jax.ShapeDtypeStruct((count, width), jnp.bfloat16),
        ],
        scratch_shapes=[
            pltpu.VMEM((4, 8, depth, width // 4), jnp.bfloat16),
            pltpu.SemaphoreType.DMA((32,)),
        ],
        compiler_params=params(24),
        name="partial",
    )(place, active, *pieces)
    block = slots // 4
    state, mix, *outgoing = pl.pallas_call(
        functools.partial(state_body, groups, experts),
        in_specs=[VMEM] * 7,
        out_specs=[VMEM] * 6,
        out_shape=[
            jax.ShapeDtypeStruct((count, width), jnp.bfloat16),
            jax.ShapeDtypeStruct((count, 32), jnp.float32),
        ]
        + [jax.ShapeDtypeStruct((block, width), jnp.bfloat16)] * 4,
        compiler_params=params(24),
        name="state",
    )(
        kept,
        swap(given, dc=1),
        residual,
        norm_gain_moe[None, :],
        routers,
        choice,
        spread,
    )

    def regrouped(blocks, which):
        return jnp.concatenate(
            [blocks[i][which * capacity : which * capacity + capacity] for i in range(4)], axis=0
        )

    passing = {0: outgoing[0]} | {d: deal(outgoing[d], d, 0) for d in NEAR[1:]}
    arrived = {d: regrouped(passing, d) for d in NEAR}
    arrived = {d: deal(arrived[d], d, 1) if d else arrived[d] for d in NEAR}
    results = {
        d: pl.pallas_call(
            experts_body,
            in_specs=[VMEM] * 4,
            out_specs=VMEM,
            out_shape=jax.ShapeDtypeStruct((block, width), jnp.bfloat16),
            compiler_params=params(16),
            name="experts",
        )(arrived[d], expert_gate_w[0], expert_up_w[0], expert_down_w[0])
        for d in NEAR
    }
    results = {d: deal(results[d], d, 1) if d else results[d] for d in NEAR}
    returned = {d: regrouped(results, d) for d in NEAR}
    returned = {d: deal(returned[d], d, 0) if d else returned[d] for d in NEAR}
    return pl.pallas_call(
        mix_body,
        in_specs=[VMEM] * 8,
        out_specs=VMEM,
        out_shape=jax.ShapeDtypeStruct((count, width), jnp.bfloat16),
        compiler_params=params(16),
        name="mix",
    )(state, first_pick, second_pick, mix, *[returned[d] for d in range(4)])


def solution(mesh):
    placed = (
        P("sp", "tp"),
        P("sp", "tp"),
        P("sp"),
        P(None, "tp"),
        P(),
        P(),
        P("tp", None),
        P(("sp", "tp"), None),
        P(),
        P(),
        P(),
        P(("sp", "tp"), None),
        P("sp", None, None),
        P("sp", None, None),
        P("sp", None, None),
    )

    return jax.shard_map(
        body, mesh=mesh, in_specs=placed, out_specs=P(("sp", "tp"), None), check_vma=False
    )
```

profile of v0, /device:TPU:1, one launch (start us, length us, event | category | flops | bytes accessed | tf_op | source)
XLA Modules:
  0.0 155.3 jit_solution(3816168596235452309)
XLA Ops:
  1.1 7.8 %collective-permute-start.9 = (bf16[1,128,128]{2,1,0:T(8,128)(2,1)S(1)}, bf16[1,128,128]{2,1,0:T(8,128)(2,1)S(1)}, u32[]{:S(2)}, u32[]{:S(2)}) collective-permute-start(bf16[1,128,128]{2,1,0:T(8,128)(2,1)S(1)} %dynamic-slice_bitcast_fusion), channel_id=1, source_target_pairs={{0,8},{1,9},{2,10},{3,11},{4,12},{5,13},{6,14},{7,15},{8,0},{9,1},... | collective-permute-start | bytes 98312 | tf_op jit(solution)/shard_map/ppermute | solution.py:368
  8.9 1.3 collective-permute-done.9
  10.2 1.5 collective-permute-start.10
  11.7 3.3 %collective-permute-done.10 = bf16[2,128,128]{2,1,0:T(8,128)(2,1)S(1)} collective-permute-done((bf16[2,128,128]{2,1,0:T(8,128)(2,1)S(1)}, bf16[2,128,128]{2,1,0:T(8,128)(2,1)S(1)}, u32[]{:S(2)}, u32[]{:S(2)}) %collective-permute-start.10) | collective-permute-done | bytes 65568 | tf_op jit(solution)/shard_map/ppermute | solution.py:368
  15.2 3.7 %collective-permute-done.11 = bf16[4,128,128]{2,1,0:T(8,128)(2,1)S(1)} collective-permute-done((bf16[4,128,128]{2,1,0:T(8,128)(2,1)S(1)}, bf16[4,128,128]{2,1,0:T(8,128)(2,1)S(1)}, u32[]{:S(2)}, u32[]{:S(2)}) %collective-permute-start.11) | collective-permute-done | bytes 131104 | tf_op jit(solution)/shard_map/ppermute | solution.py:368
  19.0 1.4 collective-permute-start.12
  20.3 1.9 %collective-permute-start.13 = (bf16[8,128,128]{2,1,0:T(8,128)(2,1)S(1)}, bf16[8,128,128]{2,1,0:T(8,128)(2,1)S(1)}, u32[]{:S(2)}, u32[]{:S(2)}) collective-permute-start(bf16[8,128,128]{2,1,0:T(8,128)(2,1)S(1)} %pad_maximum_fusion.12), channel_id=1, source_target_pairs={{0,48},{1,193},{2,50},{3,195},{4,52},{5,197},{6,54},{7,199},{8,56}... | collective-permute-start | bytes 786440 | tf_op jit(solution)/shard_map/ppermute | solution.py:373
  23.0 1.3 collective-permute-done.12
  24.3 4.0 %collective-permute-done.13 = bf16[8,128,128]{2,1,0:T(8,128)(2,1)S(1)} collective-permute-done((bf16[8,128,128]{2,1,0:T(8,128)(2,1)S(1)}, bf16[8,128,128]{2,1,0:T(8,128)(2,1)S(1)}, u32[]{:S(2)}, u32[]{:S(2)}) %collective-permute-start.13) | collective-permute-done | bytes 262176 | tf_op jit(solution)/shard_map/ppermute | solution.py:373
  28.4 1.2 collective-permute-done.14
  30.5 2.7 %collective-permute-start.17 = (bf16[4,4,128,128]{3,2,1,0:T(8,128)(2,1)S(1)}, bf16[4,4,128,128]{3,2,1,0:T(8,128)(2,1)}, u32[]{:S(2)}, u32[]{:S(2)}) collective-permute-start(bf16[4,4,128,128]{3,2,1,0:T(8,128)(2,1)S(1)} %get-tuple-element.48.high_ref), channel_id=1, source_target_pairs={{0,192},{1,49},{2,194},{3,51},{4,196},{5,53},{6,198},{7,55},{8,200... | collective-permute-start | bytes 1572872 | tf_op jit(solution)/shard_map/ppermute | solution.py:373
  34.9 3.4 %collective-permute-start = (bf16[64,128]{1,0:T(8,128)(2,1)S(1)}, bf16[64,128]{1,0:T(8,128)(2,1)S(1)}, u32[]{:S(2)}, u32[]{:S(2)}) collective-permute-start(bf16[64,128]{1,0:T(8,128)(2,1)S(1)} %tail.1), channel_id=1, source_target_pairs={{0,16},{16,32},{32,48},{48,64},{64,80},{80,96},{96,112},{112,128},... | collective-permute-start | bytes 49160 | tf_op jit(solution)/shard_map/ppermute | solution.py:391
  38.3 1.6 %collective-permute-done.17.high_3_ref = bf16[4,4,128,128]{3,2,1,0:T(8,128)(2,1)} collective-permute-done((bf16[4,4,128,128]{3,2,1,0:T(8,128)(2,1)S(1)}, bf16[4,4,128,128]{3,2,1,0:T(8,128)(2,1)}, u32[]{:S(2)}, u32[]{:S(2)}) %collective-permute-start.17) | collective-permute-done | bytes 524320 | tf_op jit(solution)/shard_map/ppermute | solution.py:373
  39.9 2.3 %pad_maximum_fusion.1 = bf16[2,4,4,128,128]{4,3,2,1,0:T(8,128)(2,1)} fusion(bf16[1,4,4,128,128]{4,3,2,1,0:T(8,128)(2,1)} %bitcast.20, bf16[1,4,4,128,128]{4,3,2,1,0:T(8,128)(2,1)} %get-tuple-element.47), kind=kLoop, calls=%fused_computation.1 | loop fusion | flops 524288 | bytes 2097152 | tf_op jit(solution)/shard_map/stack | solution.py:445
  42.5 2.1 %pad_maximum_fusion = bf16[2,4,4,128,128]{4,3,2,1,0:T(8,128)(2,1)} fusion(bf16[1,4,4,128,128]{4,3,2,1,0:T(8,128)(2,1)} %bitcast.14, bf16[1,4,4,128,128]{4,3,2,1,0:T(8,128)(2,1)S(1)} %copy-done.13), kind=kLoop, calls=%fused_computation | loop fusion | flops 524288 | bytes 2097152 | tf_op jit(solution)/shard_map/stack | solution.py:444
  44.6 2.6 %collective-permute-start.16 = (bf16[2,4,4,128,128]{4,3,2,1,0:T(8,128)(2,1)}, bf16[2,4,4,128,128]{4,3,2,1,0:T(8,128)(2,1)}, u32[]{:S(2)}, u32[]{:S(2)}) collective-permute-start(bf16[2,4,4,128,128]{4,3,2,1,0:T(8,128)(2,1)} %pad_maximum_fusion), channel_id=1, source_target_pairs={{0,192},{1,49},{2,194},{3,51},{4,196},{5,53},{6,198},{7,55},{8,200... | collective-permute-start | bytes 3145736 | tf_op jit(solution)/shard_map/ppermute | solution.py:373
  47.9 5.4 %gated_conv.1 = (bf16[384,128]{1,0:T(8,128)(2,1)S(1)}, bf16[384,128]{1,0:T(8,128)(2,1)S(1)}, bf16[384,128]{1,0:T(8,128)(2,1)S(1)}, bf16[384,128]{1,0:T(8,128)(2,...) custom-call(s32[6]{0:T(128)S(1)} %stack.78.place_ref, ...), custom_call_target="tpu_custom_call" | custom-call | tf_op jit(solution)/shard_map/gated_conv/pallas_call | solution.py:122
  53.3 5.8 %collective-permute-start.1 = (bf16[384,128]{1,0:T(8,128)(2,1)S(1)}, bf16[384,128]{1,0:T(8,128)(2,1)S(1)}, u32[]{:S(2)}, u32[]{:S(2)}) collective-permute-start(bf16[384,128]{1,0:T(8,128)(2,1)S(1)} %get-tuple-element.26), channel_id=1, source_target_pairs={{0,8},{1,9},{2,10},{3,11},{4,12},{5,13},{6,14},{7,15},{8,0},{9,1},... | collective-permute-start | bytes 294920 | tf_op jit(solution)/shard_map/ppermute | solution.py:368
  59.5 1.6 %collective-permute-done.1.refs_1_ = bf16[384,128]{1,0:T(8,128)(2,1)S(1)} collective-permute-done((bf16[384,128]{1,0:T(8,128)(2,1)S(1)}, bf16[384,128]{1,0:T(8,128)(2,1)S(1)}, u32[]{:S(2)}, u32[]{:S(2)}) %collective-permute-start.1) | collective-permute-done | bytes 98336 | tf_op jit(solution)/shard_map/ppermute | solution.py:368
  61.2 3.8 %collective-permute-done.2.refs_2_ = bf16[384,128]{1,0:T(8,128)(2,1)S(1)} collective-permute-done((bf16[384,128]{1,0:T(8,128)(2,1)S(1)}, bf16[384,128]{1,0:T(8,128)(2,1)S(1)}, u32[]{:S(2)}, u32[]{:S(2)}) %collective-permute-start.2) | collective-permute-done | bytes 98336 | tf_op jit(solution)/shard_map/ppermute | solution.py:368
  65.0 2.0 %collective-permute-start.5 = (bf16[384,128]{1,0:T(8,128)(2,1)S(1)}, bf16[384,128]{1,0:T(8,128)(2,1)S(1)}, u32[]{:S(2)}, u32[]{:S(2)}) collective-permute-start(bf16[384,128]{1,0:T(8,128)(2,1)S(1)} %get-tuple-element.30), channel_id=1, source_target_pairs={{0,10},{1,11},{2,8},{3,9},{4,14},{5,15},{6,12},{7,13},{8,2},{9,3},... | collective-permute-start | bytes 294920 | tf_op jit(solution)/shard_map/ppermute | solution.py:368
  67.0 1.2 collective-permute-start.6
  68.2 1.9 %collective-permute-start.7 = (bf16[384,128]{1,0:T(8,128)(2,1)S(1)}, bf16[384,128]{1,0:T(8,128)(2,1)S(1)}, u32[]{:S(2)}, u32[]{:S(2)}) collective-permute-start(bf16[384,128]{1,0:T(8,128)(2,1)S(1)} %get-tuple-element.32), channel_id=1, source_target_pairs={{0,14},{1,15},{2,12},{3,13},{4,10},{5,11},{6,8},{7,9},{8,6},{9,7},... | collective-permute-start | bytes 294920 | tf_op jit(solution)/shard_map/ppermute | solution.py:368
  70.2 4.0 %collective-permute-done.5.refs_5_ = bf16[384,128]{1,0:T(8,128)(2,1)S(1)} collective-permute-done((bf16[384,128]{1,0:T(8,128)(2,1)S(1)}, bf16[384,128]{1,0:T(8,128)(2,1)S(1)}, u32[]{:S(2)}, u32[]{:S(2)}) %collective-permute-start.5) | collective-permute-done | bytes 98336 | tf_op jit(solution)/shard_map/ppermute | solution.py:368
  74.8 1.8 %collective-permute-done.7.refs_7_ = bf16[384,128]{1,0:T(8,128)(2,1)S(1)} collective-permute-done((bf16[384,128]{1,0:T(8,128)(2,1)S(1)}, bf16[384,128]{1,0:T(8,128)(2,1)S(1)}, u32[]{:S(2)}, u32[]{:S(2)}) %collective-permute-start.7) | collective-permute-done | bytes 98336 | tf_op jit(solution)/shard_map/ppermute | solution.py:368
  77.1 10.0 %collective-permute-start.8 = (f32[384,128]{1,0:T(8,128)S(1)}, f32[384,128]{1,0:T(8,128)S(1)}, u32[]{:S(2)}, u32[]{:S(2)}) collective-permute-start(f32[384,128]{1,0:T(8,128)S(1)} %stats.1.mine_ref), channel_id=1, source_target_pairs={{0,1},{1,0},{2,3},{3,2},{4,5},{5,4},{6,7},{7,6},{8,9},{9,8},{10,11... | collective-permute-start | bytes 589832 | tf_op jit(solution)/shard_map/ppermute | solution.py:368
  89.4 4.0 %partial.1 = (f32[192,2048]{1,0:T(8,128)S(1)}, bf16[192,2048]{1,0:T(8,128)(2,1)S(1)}) custom-call(s32[6]{0:T(128)S(1)} %stack.78.place_ref, bf16[384,1024]{1,0:T(8,128)(2,1)S(1)} %activate.1.active_ref, bf16[4,4,128,128]{3,2,1,0:T(8,128)(2,1)S(1)} %get-tuple-element.50.low_ref, bf16[4,4,128,128]{3,2,1,0:T(8,128)(2,1)} %collective-permute-done.15.low_1_ref, ...), custom_call_target="tpu_custom_call" | custom-call | tf_op jit(solution)/shard_map/partial/pallas_call | solution.py:507
  95.8 1.3 state.1
  97.2 1.7 %collective-permute-start.21 = (bf16[96,2048]{1,0:T(8,128)(2,1)S(1)}, bf16[96,2048]{1,0:T(8,128)(2,1)S(1)}, u32[]{:S(2)}, u32[]{:S(2)}) collective-permute-start(bf16[96,2048]{1,0:T(8,128)(2,1)S(1)} %get-tuple-element.43), channel_id=1, source_target_pairs={{0,32},{1,129},{2,34},{3,131},{4,36},{5,133},{6,38},{7,135},{8,40}... | collective-permute-start | bytes 1179656 | tf_op jit(solution)/shard_map/ppermute | solution.py:385
  98.9 2.7 %collective-permute-start.22 = (bf16[96,2048]{1,0:T(8,128)(2,1)S(1)}, bf16[96,2048]{1,0:T(8,128)(2,1)S(1)}, u32[]{:S(2)}, u32[]{:S(2)}) collective-permute-start(bf16[96,2048]{1,0:T(8,128)(2,1)S(1)} %get-tuple-element.44), channel_id=1, source_target_pairs={{0,49},{1,192},{2,51},{3,194},{4,53},{5,196},{6,55},{7,198},{8,57}... | collective-permute-start | bytes 1179656 | tf_op jit(solution)/shard_map/ppermute | solution.py:385
  101.7 3.0 %collective-permute-done.20 = bf16[96,2048]{1,0:T(8,128)(2,1)S(1)} collective-permute-done((bf16[96,2048]{1,0:T(8,128)(2,1)S(1)}, bf16[96,2048]{1,0:T(8,128)(2,1)S(1)}, u32[]{:S(2)}, u32[]{:S(2)}) %collective-permute-start.20) | collective-permute-done | bytes 393248 | tf_op jit(solution)/shard_map/ppermute | solution.py:385
  104.8 3.8 %collective-permute-done.21 = bf16[96,2048]{1,0:T(8,128)(2,1)S(1)} collective-permute-done((bf16[96,2048]{1,0:T(8,128)(2,1)S(1)}, bf16[96,2048]{1,0:T(8,128)(2,1)S(1)}, u32[]{:S(2)}, u32[]{:S(2)}) %collective-permute-start.21) | collective-permute-done | bytes 393248 | tf_op jit(solution)/shard_map/ppermute | solution.py:385
  108.6 3.3 %collective-permute-done.22 = bf16[96,2048]{1,0:T(8,128)(2,1)S(1)} collective-permute-done((bf16[96,2048]{1,0:T(8,128)(2,1)S(1)}, bf16[96,2048]{1,0:T(8,128)(2,1)S(1)}, u32[]{:S(2)}, u32[]{:S(2)}) %collective-permute-start.22) | collective-permute-done | bytes 393248 | tf_op jit(solution)/shard_map/ppermute | solution.py:385
  112.1 2.2 %collective-permute-start.25 = (bf16[96,2048]{1,0:T(8,128)(2,1)S(1)}, bf16[96,2048]{1,0:T(8,128)(2,1)S(1)}, u32[]{:S(2)}, u32[]{:S(2)}) collective-permute-start(bf16[96,2048]{1,0:T(8,128)(2,1)S(1)} %pad_maximum_fusion.6), channel_id=1, source_target_pairs={{0,128},{1,33},{2,130},{3,35},{4,132},{5,37},{6,134},{7,39},{8,136... | collective-permute-start | bytes 1179656 | tf_op jit(solution)/shard_map/ppermute | solution.py:385
  114.3 2.4 %collective-permute-start.27 = (bf16[96,2048]{1,0:T(8,128)(2,1)S(1)}, bf16[96,2048]{1,0:T(8,128)(2,1)S(1)}, u32[]{:S(2)}, u32[]{:S(2)}) collective-permute-start(bf16[96,2048]{1,0:T(8,128)(2,1)S(1)} %pad_maximum_fusion.7), channel_id=1, source_target_pairs={{0,193},{1,48},{2,195},{3,50},{4,197},{5,52},{6,199},{7,54},{8,201... | collective-permute-start | bytes 1179656 | tf_op jit(solution)/shard_map/ppermute | solution.py:385
  116.7 1.2 experts.4
  117.9 1.6 %collective-permute-done.23.rows_ref = bf16[96,2048]{1,0:T(8,128)(2,1)S(1)} collective-permute-done((bf16[96,2048]{1,0:T(8,128)(2,1)S(1)}, bf16[96,2048]{1,0:T(8,128)(2,1)S(1)}, u32[]{:S(2)}, u32[]{:S(2)}) %collective-permute-start.23) | collective-permute-done | bytes 393248 | tf_op jit(solution)/shard_map/ppermute | solution.py:385
  119.5 1.2 experts.5
  120.9 3.0 %collective-permute-done.25.rows_ref = bf16[96,2048]{1,0:T(8,128)(2,1)S(1)} collective-permute-done((bf16[96,2048]{1,0:T(8,128)(2,1)S(1)}, bf16[96,2048]{1,0:T(8,128)(2,1)S(1)}, u32[]{:S(2)}, u32[]{:S(2)}) %collective-permute-start.25) | collective-permute-done | bytes 393248 | tf_op jit(solution)/shard_map/ppermute | solution.py:385
  123.9 1.2 experts.6
  125.1 1.2 collective-permute-start.26
  127.0 1.2 experts.7
  128.2 2.3 %collective-permute-start.28 = (bf16[96,2048]{1,0:T(8,128)(2,1)S(1)}, bf16[96,2048]{1,0:T(8,128)(2,1)S(1)}, u32[]{:S(2)}, u32[]{:S(2)}) collective-permute-start(bf16[96,2048]{1,0:T(8,128)(2,1)S(1)} %experts.7), channel_id=1, source_target_pairs={{0,193},{1,48},{2,195},{3,50},{4,197},{5,52},{6,199},{7,54},{8,201... | collective-permute-start | bytes 1179656 | tf_op jit(solution)/shard_map/ppermute | solution.py:385
  130.6 3.2 %collective-permute-done.26 = bf16[96,2048]{1,0:T(8,128)(2,1)S(1)} collective-permute-done((bf16[96,2048]{1,0:T(8,128)(2,1)S(1)}, bf16[96,2048]{1,0:T(8,128)(2,1)S(1)}, u32[]{:S(2)}, u32[]{:S(2)}) %collective-permute-start.26) | collective-permute-done | bytes 393248 | tf_op jit(solution)/shard_map/ppermute | solution.py:385
  133.8 4.2 %collective-permute-done.28 = bf16[96,2048]{1,0:T(8,128)(2,1)S(1)} collective-permute-done((bf16[96,2048]{1,0:T(8,128)(2,1)S(1)}, bf16[96,2048]{1,0:T(8,128)(2,1)S(1)}, u32[]{:S(2)}, u32[]{:S(2)}) %collective-permute-start.28) | collective-permute-done | bytes 393248 | tf_op jit(solution)/shard_map/ppermute | solution.py:385
  138.1 4.5 %collective-permute-start.31 = (bf16[96,2048]{1,0:T(8,128)(2,1)S(1)}, bf16[96,2048]{1,0:T(8,128)(2,1)S(1)}, u32[]{:S(2)}, u32[]{:S(2)}) collective-permute-start(bf16[96,2048]{1,0:T(8,128)(2,1)S(1)} %pad_maximum_fusion.11), channel_id=1, source_target_pairs={{0,49},{1,192},{2,51},{3,194},{4,53},{5,196},{6,55},{7,198},{8,57}... | collective-permute-start | bytes 1179656 | tf_op jit(solution)/shard_map/ppermute | solution.py:385
  143.8 8.5 %collective-permute-done.31.refs_3_ = bf16[96,2048]{1,0:T(8,128)(2,1)S(1)} collective-permute-done((bf16[96,2048]{1,0:T(8,128)(2,1)S(1)}, bf16[96,2048]{1,0:T(8,128)(2,1)S(1)}, u32[]{:S(2)}, u32[]{:S(2)}) %collective-permute-start.31) | collective-permute-done | bytes 393248 | tf_op jit(solution)/shard_map/ppermute | solution.py:385
  153.3 1.9 %mix.1 = bf16[192,2048]{1,0:T(8,128)(2,1)} custom-call(bf16[192,2048]{1,0:T(8,128)(2,1)S(1)} %get-tuple-element.37.state_ref, bf16[192,384]{1,0:T(8,128)(2,1)S(1)} %get-tuple-element.38.first_ref, bf16[192,384]{1,0:T(8,128)(2,1)S(1)} %get-tuple-element.39.second_ref, f32[192,32]{1,0:T(8,128)S(1)} %get-tuple-element.40.mix_ref, ...), custom_call_target="tpu_custom_call" | custom-call | tf_op jit(solution)/shard_map/mix/pallas_call | solution.py:566
  (98 shorter events, 15.3 us)
Async XLA Ops:
  0.0 1.0 copy-start
  1.1 9.1 %collective-permute-start.9 = (bf16[1,128,128]{2,1,0:T(8,128)(2,1)S(1)}, bf16[1,128,128]{2,1,0:T(8,128)(2,1)S(1)}, u32[]{:S(2)}, u32[]{:S(2)}) collective-permute-start(bf16[1,128,128]{2,1,0:T(8,128)(2,1)S(1)} %dynamic-slice_bitcast_fusion), channel_id=1, source_target_pairs={{0,8},{1,9},{2,10},{3,11},{4,12},{5,13},{6,14},{7,15},{8,0},{9,1},... | collective-permute-start | bytes 98312 | tf_op jit(solution)/shard_map/ppermute | solution.py:368
  10.2 4.8 %collective-permute-start.10 = (bf16[2,128,128]{2,1,0:T(8,128)(2,1)S(1)}, bf16[2,128,128]{2,1,0:T(8,128)(2,1)S(1)}, u32[]{:S(2)}, u32[]{:S(2)}) collective-permute-start(bf16[2,128,128]{2,1,0:T(8,128)(2,1)S(1)} %pad_maximum_fusion.14), channel_id=1, source_target_pairs={{0,4},{1,5},{2,6},{3,7},{4,0},{5,1},{6,2},{7,3},{8,12},{9,13},{10,... | collective-permute-start | bytes 196616 | tf_op jit(solution)/shard_map/ppermute | solution.py:368
  15.0 3.9 %collective-permute-start.11 = (bf16[4,128,128]{2,1,0:T(8,128)(2,1)S(1)}, bf16[4,128,128]{2,1,0:T(8,128)(2,1)S(1)}, u32[]{:S(2)}, u32[]{:S(2)}) collective-permute-start(bf16[4,128,128]{2,1,0:T(8,128)(2,1)S(1)} %get-tuple-element.90), channel_id=1, source_target_pairs={{0,2},{1,3},{2,0},{3,1},{4,6},{5,7},{6,4},{7,5},{8,10},{9,11},{10,... | collective-permute-start | bytes 393224 | tf_op jit(solution)/shard_map/ppermute | solution.py:368
  19.0 5.3 %collective-permute-start.12 = (bf16[8,128,128]{2,1,0:T(8,128)(2,1)S(1)}, bf16[8,128,128]{2,1,0:T(8,128)(2,1)S(1)}, u32[]{:S(2)}, u32[]{:S(2)}) collective-permute-start(bf16[8,128,128]{2,1,0:T(8,128)(2,1)S(1)} %pad_maximum_fusion.12), channel_id=1, source_target_pairs={{0,16},{1,65},{2,18},{3,67},{4,20},{5,69},{6,22},{7,71},{8,24},{9,... | collective-permute-start | bytes 786440 | tf_op jit(solution)/shard_map/ppermute | solution.py:373
  20.3 8.0 %collective-permute-start.13 = (bf16[8,128,128]{2,1,0:T(8,128)(2,1)S(1)}, bf16[8,128,128]{2,1,0:T(8,128)(2,1)S(1)}, u32[]{:S(2)}, u32[]{:S(2)}) collective-permute-start(bf16[8,128,128]{2,1,0:T(8,128)(2,1)S(1)} %pad_maximum_fusion.12), channel_id=1, source_target_pairs={{0,48},{1,193},{2,50},{3,195},{4,52},{5,197},{6,54},{7,199},{8,56}... | collective-permute-start | bytes 786440 | tf_op jit(solution)/shard_map/ppermute | solution.py:373
  22.2 7.3 %collective-permute-start.14 = (bf16[8,128,128]{2,1,0:T(8,128)(2,1)S(1)}, bf16[8,128,128]{2,1,0:T(8,128)(2,1)S(1)}, u32[]{:S(2)}, u32[]{:S(2)}) collective-permute-start(bf16[8,128,128]{2,1,0:T(8,128)(2,1)S(1)} %pad_maximum_fusion.12), channel_id=1, source_target_pairs={{0,32},{1,129},{2,34},{3,131},{4,36},{5,133},{6,38},{7,135},{8,40}... | collective-permute-start | bytes 786440 | tf_op jit(solution)/shard_map/ppermute | solution.py:373
  24.3 9.8 %copy-start.4 = (bf16[3072,128]{1,0:T(8,128)(2,1)S(1)}, bf16[3072,128]{1,0:T(8,128)(2,1)}, u32[]{:S(2)}) copy-start(bf16[3072,128]{1,0:T(8,128)(2,1)} %value_halo_ref.1) | copy-start | bytes 2359300
  24.3 9.8 %copy-start.5 = (bf16[3072,128]{1,0:T(8,128)(2,1)S(1)}, bf16[3072,128]{1,0:T(8,128)(2,1)}, u32[]{:S(2)}) copy-start(bf16[3072,128]{1,0:T(8,128)(2,1)} %gate_halo_ref.1) | copy-start | bytes 2359300
  24.3 9.8 %copy-start.7 = (s32[3072]{0:T(1024)S(1)}, s32[3072]{0:T(1024)}, u32[]{:S(2)}) copy-start(s32[3072]{0:T(1024)} %ids_ref.1) | copy-start | bytes 36868
  30.5 9.4 %collective-permute-start.17 = (bf16[4,4,128,128]{3,2,1,0:T(8,128)(2,1)S(1)}, bf16[4,4,128,128]{3,2,1,0:T(8,128)(2,1)}, u32[]{:S(2)}, u32[]{:S(2)}) collective-permute-start(bf16[4,4,128,128]{3,2,1,0:T(8,128)(2,1)S(1)} %get-tuple-element.48.high_ref), channel_id=1, source_target_pairs={{0,192},{1,49},{2,194},{3,51},{4,196},{5,53},{6,198},{7,55},{8,200... | collective-permute-start | bytes 1572872 | tf_op jit(solution)/shard_map/ppermute | solution.py:373
  34.1 8.4 %collective-permute-start.15 = (bf16[4,4,128,128]{3,2,1,0:T(8,128)(2,1)S(1)}, bf16[4,4,128,128]{3,2,1,0:T(8,128)(2,1)}, u32[]{:S(2)}, u32[]{:S(2)}) collective-permute-start(bf16[4,4,128,128]{3,2,1,0:T(8,128)(2,1)S(1)} %get-tuple-element.50.low_ref), channel_id=1, source_target_pairs={{0,64},{1,17},{2,66},{3,19},{4,68},{5,21},{6,70},{7,23},{8,72},{9,... | collective-permute-start | bytes 1572872 | tf_op jit(solution)/shard_map/ppermute | solution.py:373
  34.9 12.7 %collective-permute-start = (bf16[64,128]{1,0:T(8,128)(2,1)S(1)}, bf16[64,128]{1,0:T(8,128)(2,1)S(1)}, u32[]{:S(2)}, u32[]{:S(2)}) collective-permute-start(bf16[64,128]{1,0:T(8,128)(2,1)S(1)} %tail.1), channel_id=1, source_target_pairs={{0,16},{16,32},{32,48},{48,64},{64,80},{80,96},{96,112},{112,128},... | collective-permute-start | bytes 49160 | tf_op jit(solution)/shard_map/ppermute | solution.py:391
  38.2 4.3 %copy-start.13 = (bf16[1,4,4,128,128]{4,3,2,1,0:T(8,128)(2,1)S(1)}, bf16[1,4,4,128,128]{4,3,2,1,0:T(8,128)(2,1)}, u32[]{:S(2)}) copy-start(bf16[1,4,4,128,128]{4,3,2,1,0:T(8,128)(2,1)} %get-tuple-element.49) | copy-start | bytes 1572868
  39.9 8.0 %copy-start.8 = (bf16[31,128]{1,0:T(8,128)(2,1)S(1)}, bf16[31,128]{1,0:T(8,128)(2,1)}, u32[]{:S(2)}) copy-start(bf16[31,128]{1,0:T(8,128)(2,1)} %kernel_ref.1) | copy-start | bytes 23812
  42.2 47.2 %collective-permute-start.18 = (bf16[2,4,4,128,128]{4,3,2,1,0:T(8,128)(2,1)}, bf16[2,4,4,128,128]{4,3,2,1,0:T(8,128)(2,1)}, u32[]{:S(2)}, u32[]{:S(2)}) collective-permute-start(bf16[2,4,4,128,128]{4,3,2,1,0:T(8,128)(2,1)} %pad_maximum_fusion.1), channel_id=1, source_target_pairs={{0,64},{1,17},{2,66},{3,19},{4,68},{5,21},{6,70},{7,23},{8,72},{9,... | collective-permute-start | bytes 3145736 | tf_op jit(solution)/shard_map/ppermute | solution.py:373
  44.6 44.7 %collective-permute-start.16 = (bf16[2,4,4,128,128]{4,3,2,1,0:T(8,128)(2,1)}, bf16[2,4,4,128,128]{4,3,2,1,0:T(8,128)(2,1)}, u32[]{:S(2)}, u32[]{:S(2)}) collective-permute-start(bf16[2,4,4,128,128]{4,3,2,1,0:T(8,128)(2,1)} %pad_maximum_fusion), channel_id=1, source_target_pairs={{0,192},{1,49},{2,194},{3,51},{4,196},{5,53},{6,198},{7,55},{8,200... | collective-permute-start | bytes 3145736 | tf_op jit(solution)/shard_map/ppermute | solution.py:373
  47.8 40.4 %copy-start.9 = (f32[2048]{0:T(1024)S(1)}, f32[2048]{0:T(1024)}, u32[]{:S(2)}) copy-start(f32[2048]{0:T(1024)} %param.19) | copy-start | bytes 24580
  47.8 40.4 %copy-start.10 = (f32[2048]{0:T(1024)S(1)}, f32[2048]{0:T(1024)}, u32[]{:S(2)}) copy-start(f32[2048]{0:T(1024)} %param.20) | copy-start | bytes 24580
  53.3 7.8 %collective-permute-start.1 = (bf16[384,128]{1,0:T(8,128)(2,1)S(1)}, bf16[384,128]{1,0:T(8,128)(2,1)S(1)}, u32[]{:S(2)}, u32[]{:S(2)}) collective-permute-start(bf16[384,128]{1,0:T(8,128)(2,1)S(1)} %get-tuple-element.26), channel_id=1, source_target_pairs={{0,8},{1,9},{2,10},{3,11},{4,12},{5,13},{6,14},{7,15},{8,0},{9,1},... | collective-permute-start | bytes 294920 | tf_op jit(solution)/shard_map/ppermute | solution.py:368
  59.1 5.8 %collective-permute-start.2 = (bf16[384,128]{1,0:T(8,128)(2,1)S(1)}, bf16[384,128]{1,0:T(8,128)(2,1)S(1)}, u32[]{:S(2)}, u32[]{:S(2)}) collective-permute-start(bf16[384,128]{1,0:T(8,128)(2,1)S(1)} %get-tuple-element.27), channel_id=1, source_target_pairs={{0,4},{1,5},{2,6},{3,7},{4,0},{5,1},{6,2},{7,3},{8,12},{9,13},{10,... | collective-permute-start | bytes 294920 | tf_op jit(solution)/shard_map/ppermute | solution.py:368
  59.2 7.9 %collective-permute-start.3 = (bf16[384,128]{1,0:T(8,128)(2,1)S(1)}, bf16[384,128]{1,0:T(8,128)(2,1)S(1)}, u32[]{:S(2)}, u32[]{:S(2)}) collective-permute-start(bf16[384,128]{1,0:T(8,128)(2,1)S(1)} %get-tuple-element.28), channel_id=1, source_target_pairs={{0,12},{1,13},{2,14},{3,15},{4,8},{5,9},{6,10},{7,11},{8,4},{9,5},... | collective-permute-start | bytes 294920 | tf_op jit(solution)/shard_map/ppermute | solution.py:368
  61.2 7.1 %collective-permute-start.4 = (bf16[384,128]{1,0:T(8,128)(2,1)S(1)}, bf16[384,128]{1,0:T(8,128)(2,1)S(1)}, u32[]{:S(2)}, u32[]{:S(2)}) collective-permute-start(bf16[384,128]{1,0:T(8,128)(2,1)S(1)} %get-tuple-element.29), channel_id=1, source_target_pairs={{0,2},{1,3},{2,0},{3,1},{4,6},{5,7},{6,4},{7,5},{8,10},{9,11},{10,... | collective-permute-start | bytes 294920 | tf_op jit(solution)/shard_map/ppermute | solution.py:368
  65.0 9.2 %collective-permute-start.5 = (bf16[384,128]{1,0:T(8,128)(2,1)S(1)}, bf16[384,128]{1,0:T(8,128)(2,1)S(1)}, u32[]{:S(2)}, u32[]{:S(2)}) collective-permute-start(bf16[384,128]{1,0:T(8,128)(2,1)S(1)} %get-tuple-element.30), channel_id=1, source_target_pairs={{0,10},{1,11},{2,8},{3,9},{4,14},{5,15},{6,12},{7,13},{8,2},{9,3},... | collective-permute-start | bytes 294920 | tf_op jit(solution)/shard_map/ppermute | solution.py:368
  67.0 7.8 %collective-permute-start.6 = (bf16[384,128]{1,0:T(8,128)(2,1)S(1)}, bf16[384,128]{1,0:T(8,128)(2,1)S(1)}, u32[]{:S(2)}, u32[]{:S(2)}) collective-permute-start(bf16[384,128]{1,0:T(8,128)(2,1)S(1)} %get-tuple-element.31), channel_id=1, source_target_pairs={{0,6},{1,7},{2,4},{3,5},{4,2},{5,3},{6,0},{7,1},{8,14},{9,15},{10,... | collective-permute-start | bytes 294920 | tf_op jit(solution)/shard_map/ppermute | solution.py:368
  68.2 8.4 %collective-permute-start.7 = (bf16[384,128]{1,0:T(8,128)(2,1)S(1)}, bf16[384,128]{1,0:T(8,128)(2,1)S(1)}, u32[]{:S(2)}, u32[]{:S(2)}) collective-permute-start(bf16[384,128]{1,0:T(8,128)(2,1)S(1)} %get-tuple-element.32), channel_id=1, source_target_pairs={{0,14},{1,15},{2,12},{3,13},{4,10},{5,11},{6,8},{7,9},{8,6},{9,7},... | collective-permute-start | bytes 294920 | tf_op jit(solution)/shard_map/ppermute | solution.py:368
  77.1 11.1 %collective-permute-start.8 = (f32[384,128]{1,0:T(8,128)S(1)}, f32[384,128]{1,0:T(8,128)S(1)}, u32[]{:S(2)}, u32[]{:S(2)}) collective-permute-start(f32[384,128]{1,0:T(8,128)S(1)} %stats.1.mine_ref), channel_id=1, source_target_pairs={{0,1},{1,0},{2,3},{3,2},{4,5},{5,4},{6,7},{7,6},{8,9},{9,8},{10,11... | collective-permute-start | bytes 589832 | tf_op jit(solution)/shard_map/ppermute | solution.py:368
  89.3 4.6 %copy-start.12 = (s32[192,2]{0,1:T(2,128)S(1)}, s32[192,2]{0,1:T(2,128)}, u32[]{:S(2)}) copy-start(s32[192,2]{0,1:T(2,128)} %param.26) | copy-start | bytes 4612
  89.3 5.6 %copy-start.14 = (bf16[2048,16]{0,1:T(8,128)(2,1)S(1)}, bf16[2048,16]{0,1:T(8,128)(2,1)}, u32[]{:S(2)}) copy-start(bf16[2048,16]{0,1:T(8,128)(2,1)} %param.25) | copy-start | bytes 196612
  89.3 5.6 %copy-start.15 = (bf16[2048,2]{0,1:T(2,128)(2,1)S(1)}, bf16[2048,2]{0,1:T(2,128)(2,1)}, u32[]{:S(2)}) copy-start(bf16[2048,2]{0,1:T(2,128)(2,1)} %param.24) | copy-start | bytes 24580
  89.3 6.5 %copy-start.6 = (bf16[192,2048]{1,0:T(8,128)(2,1)S(1)}, bf16[192,2048]{1,0:T(8,128)(2,1)}, u32[]{:S(2)}) copy-start(bf16[192,2048]{1,0:T(8,128)(2,1)} %residual_ref.1) | copy-start | bytes 2359300
  89.3 6.5 %copy-start.11 = (f32[2048]{0:T(1024)S(1)}, f32[2048]{0:T(1024)}, u32[]{:S(2)}) copy-start(f32[2048]{0:T(1024)} %param.23) | copy-start | bytes 24580
  93.4 2.4 %collective-permute-start.19 = (bf16[192,2048]{1,0:T(8,128)(2,1)S(1)}, bf16[192,2048]{1,0:T(8,128)(2,1)S(1)}, u32[]{:S(2)}, u32[]{:S(2)}) collective-permute-start(bf16[192,2048]{1,0:T(8,128)(2,1)S(1)} %get-tuple-element.34), channel_id=1, source_target_pairs={{0,1},{1,0},{2,3},{3,2},{4,5},{5,4},{6,7},{7,6},{8,9},{9,8},{10,11... | collective-permute-start | bytes 2359304 | tf_op jit(solution)/shard_map/ppermute | solution.py:368
  97.1 7.6 %collective-permute-start.20 = (bf16[96,2048]{1,0:T(8,128)(2,1)S(1)}, bf16[96,2048]{1,0:T(8,128)(2,1)S(1)}, u32[]{:S(2)}, u32[]{:S(2)}) collective-permute-start(bf16[96,2048]{1,0:T(8,128)(2,1)S(1)} %get-tuple-element.42), channel_id=1, source_target_pairs={{0,17},{1,64},{2,19},{3,66},{4,21},{5,68},{6,23},{7,70},{8,25},{9,... | collective-permute-start | bytes 1179656 | tf_op jit(solution)/shard_map/ppermute | solution.py:385
  97.2 11.3 %collective-permute-start.21 = (bf16[96,2048]{1,0:T(8,128)(2,1)S(1)}, bf16[96,2048]{1,0:T(8,128)(2,1)S(1)}, u32[]{:S(2)}, u32[]{:S(2)}) collective-permute-start(bf16[96,2048]{1,0:T(8,128)(2,1)S(1)} %get-tuple-element.43), channel_id=1, source_target_pairs={{0,32},{1,129},{2,34},{3,131},{4,36},{5,133},{6,38},{7,135},{8,40}... | collective-permute-start | bytes 1179656 | tf_op jit(solution)/shard_map/ppermute | solution.py:385
  98.9 12.9 %collective-permute-start.22 = (bf16[96,2048]{1,0:T(8,128)(2,1)S(1)}, bf16[96,2048]{1,0:T(8,128)(2,1)S(1)}, u32[]{:S(2)}, u32[]{:S(2)}) collective-permute-start(bf16[96,2048]{1,0:T(8,128)(2,1)S(1)} %get-tuple-element.44), channel_id=1, source_target_pairs={{0,49},{1,192},{2,51},{3,194},{4,53},{5,196},{6,55},{7,198},{8,57}... | collective-permute-start | bytes 1179656 | tf_op jit(solution)/shard_map/ppermute | solution.py:385
  101.7 15.0 %copy-start.3 = (bf16[1,512,2048]{2,1,0:T(8,128)(2,1)S(1)}, bf16[1,512,2048]{2,1,0:T(8,128)(2,1)}, u32[]{:S(2)}) copy-start(bf16[1,512,2048]{2,1,0:T(8,128)(2,1)} %param.29) | copy-start | bytes 6291460
  108.6 8.1 %copy-start.2 = (bf16[1,2048,512]{2,1,0:T(8,128)(2,1)S(1)}, bf16[1,2048,512]{2,1,0:T(8,128)(2,1)}, u32[]{:S(2)}) copy-start(bf16[1,2048,512]{2,1,0:T(8,128)(2,1)} %param.28) | copy-start | bytes 6291460
  108.6 8.1 %copy-start.1 = (bf16[1,2048,512]{2,1,0:T(8,128)(2,1)S(1)}, bf16[1,2048,512]{2,1,0:T(8,128)(2,1)}, u32[]{:S(2)}) copy-start(bf16[1,2048,512]{2,1,0:T(8,128)(2,1)} %param.27) | copy-start | bytes 6291460
  111.9 7.6 %collective-permute-start.23 = (bf16[96,2048]{1,0:T(8,128)(2,1)S(1)}, bf16[96,2048]{1,0:T(8,128)(2,1)S(1)}, u32[]{:S(2)}, u32[]{:S(2)}) collective-permute-start(bf16[96,2048]{1,0:T(8,128)(2,1)S(1)} %pad_maximum_fusion.5), channel_id=1, source_target_pairs={{0,65},{1,16},{2,67},{3,18},{4,69},{5,20},{6,71},{7,22},{8,73},{9,... | collective-permute-start | bytes 1179656 | tf_op jit(solution)/shard_map/ppermute | solution.py:385
  112.1 11.8 %collective-permute-start.25 = (bf16[96,2048]{1,0:T(8,128)(2,1)S(1)}, bf16[96,2048]{1,0:T(8,128)(2,1)S(1)}, u32[]{:S(2)}, u32[]{:S(2)}) collective-permute-start(bf16[96,2048]{1,0:T(8,128)(2,1)S(1)} %pad_maximum_fusion.6), channel_id=1, source_target_pairs={{0,128},{1,33},{2,130},{3,35},{4,132},{5,37},{6,134},{7,39},{8,136... | collective-permute-start | bytes 1179656 | tf_op jit(solution)/shard_map/ppermute | solution.py:385
  114.3 12.7 %collective-permute-start.27 = (bf16[96,2048]{1,0:T(8,128)(2,1)S(1)}, bf16[96,2048]{1,0:T(8,128)(2,1)S(1)}, u32[]{:S(2)}, u32[]{:S(2)}) collective-permute-start(bf16[96,2048]{1,0:T(8,128)(2,1)S(1)} %pad_maximum_fusion.7), channel_id=1, source_target_pairs={{0,193},{1,48},{2,195},{3,50},{4,197},{5,52},{6,199},{7,54},{8,201... | collective-permute-start | bytes 1179656 | tf_op jit(solution)/shard_map/ppermute | solution.py:385
  120.7 9.9 %collective-permute-start.24 = (bf16[96,2048]{1,0:T(8,128)(2,1)S(1)}, bf16[96,2048]{1,0:T(8,128)(2,1)S(1)}, u32[]{:S(2)}, u32[]{:S(2)}) collective-permute-start(bf16[96,2048]{1,0:T(8,128)(2,1)S(1)} %experts.5), channel_id=1, source_target_pairs={{0,65},{1,16},{2,67},{3,18},{4,69},{5,20},{6,71},{7,22},{8,73},{9,... | collective-permute-start | bytes 1179656 | tf_op jit(solution)/shard_map/ppermute | solution.py:385
  125.1 8.7 %collective-permute-start.26 = (bf16[96,2048]{1,0:T(8,128)(2,1)S(1)}, bf16[96,2048]{1,0:T(8,128)(2,1)S(1)}, u32[]{:S(2)}, u32[]{:S(2)}) collective-permute-start(bf16[96,2048]{1,0:T(8,128)(2,1)S(1)} %experts.6), channel_id=1, source_target_pairs={{0,128},{1,33},{2,130},{3,35},{4,132},{5,37},{6,134},{7,39},{8,136... | collective-permute-start | bytes 1179656 | tf_op jit(solution)/shard_map/ppermute | solution.py:385
  128.2 9.8 %collective-permute-start.28 = (bf16[96,2048]{1,0:T(8,128)(2,1)S(1)}, bf16[96,2048]{1,0:T(8,128)(2,1)S(1)}, u32[]{:S(2)}, u32[]{:S(2)}) collective-permute-start(bf16[96,2048]{1,0:T(8,128)(2,1)S(1)} %experts.7), channel_id=1, source_target_pairs={{0,193},{1,48},{2,195},{3,50},{4,197},{5,52},{6,199},{7,54},{8,201... | collective-permute-start | bytes 1179656 | tf_op jit(solution)/shard_map/ppermute | solution.py:385
  138.1 14.2 %collective-permute-start.31 = (bf16[96,2048]{1,0:T(8,128)(2,1)S(1)}, bf16[96,2048]{1,0:T(8,128)(2,1)S(1)}, u32[]{:S(2)}, u32[]{:S(2)}) collective-permute-start(bf16[96,2048]{1,0:T(8,128)(2,1)S(1)} %pad_maximum_fusion.11), channel_id=1, source_target_pairs={{0,49},{1,192},{2,51},{3,194},{4,53},{5,196},{6,55},{7,198},{8,57}... | collective-permute-start | bytes 1179656 | tf_op jit(solution)/shard_map/ppermute | solution.py:385
  142.6 9.6 %collective-permute-start.30 = (bf16[96,2048]{1,0:T(8,128)(2,1)S(1)}, bf16[96,2048]{1,0:T(8,128)(2,1)S(1)}, u32[]{:S(2)}, u32[]{:S(2)}) collective-permute-start(bf16[96,2048]{1,0:T(8,128)(2,1)S(1)} %pad_maximum_fusion.10), channel_id=1, source_target_pairs={{0,32},{1,129},{2,34},{3,131},{4,36},{5,133},{6,38},{7,135},{8,40}... | collective-permute-start | bytes 1179656 | tf_op jit(solution)/shard_map/ppermute | solution.py:385
  142.8 10.5 %collective-permute-start.29 = (bf16[96,2048]{1,0:T(8,128)(2,1)S(1)}, bf16[96,2048]{1,0:T(8,128)(2,1)S(1)}, u32[]{:S(2)}, u32[]{:S(2)}) collective-permute-start(bf16[96,2048]{1,0:T(8,128)(2,1)S(1)} %pad_maximum_fusion.9), channel_id=1, source_target_pairs={{0,17},{1,64},{2,19},{3,66},{4,21},{5,68},{6,23},{7,70},{8,25},{9,... | collective-permute-start | bytes 1179656 | tf_op jit(solution)/shard_map/ppermute | solution.py:385
where the time goes:
time: 155 us
  starting transfers between devices  62.7 us (40%)
  waiting for transfers between devices  62.7 us (40%)
  Pallas kernels  20.9 us (13%)
  other arithmetic  6.88 us (4%)
  local copies, waits for them, and re-layouts  1.74 us (1%)
    ppermute x12, waiting for transfers between devices, deal(): return lax.ppermute(array, ('sp', 'tp'), pairs)  32.4 us
    ppermute x12, starting transfers between devices, swap(): lax.ppermute(array, ('sp', 'tp'), [(i, i ^ flip) for i in range(256)])  31.4 us
    ppermute x12, waiting for transfers between devices, swap(): lax.ppermute(array, ('sp', 'tp'), [(i, i ^ flip) for i in range(256)])  22 us
    ppermute x12, starting transfers between devices, deal(): return lax.ppermute(array, ('sp', 'tp'), pairs)  18.3 us
    ppermute x7, starting transfers between devices, cross(): return lax.ppermute(array, ('sp', 'tp'), pairs)  9.6 us
    ppermute x7, waiting for transfers between devices, cross(): return lax.ppermute(array, ('sp', 'tp'), pairs)  8.26 us
    pallas_call x1, Pallas kernels, convolve_tokens(): pl.pallas_call(conv_kernel_body, grid_spec=pltpu.PrefetchScalarGridSpec(n...  5.42 us
    pallas_call x4, Pallas kernels, body(): pl.pallas_call(experts_body, in_specs=[VMEM] * 4, out_specs=VMEM, out_sha...  4.86 us
  transfers between devices with their start and end apart: 32, of which 25 were waited for; matrix products, arithmetic and copies ran while one was open for 4% of the time, Pallas kernels for 9%

commit v1 on v0

--- a/solution.py
+++ b/solution.py
@@ -20,46 +20,22 @@
     return pltpu.CompilerParams(vmem_limit_bytes=mib * 1024 * 1024)
 
 
-def conv_kernel_body(
-    place_ref,
-    starts_ref,
-    edge_ref,
-    value_ref,
-    gate_ref,
-    value_halo_ref,
-    gate_halo_ref,
-    rim_ref,
-    kernel_ref,
-    *refs,
-):
+def conv_kernel_body(place_ref, ids_ref, ids_grid_ref, gated_ref, rim_ref, kernel_ref, *refs):
     outs, (taps, rows, masked, total) = refs[:-4], refs[-4:]
-    step = pl.program_id(0)
-    at_tile = step ^ place_ref[0]
-    tile, lanes = value_ref.shape
+    tile, lanes = outs[0].shape
     tap_count = kernel_ref.shape[0]
-
-    def gated(value, gate):
-        return (
-            (value[...].astype(jnp.float32) * jax.nn.sigmoid(gate[...].astype(jnp.float32)))
-            .astype(jnp.bfloat16)
-            .astype(jnp.float32)
-        )
-
-    @pl.when(step == 0)
-    def _():
-        kernel = kernel_ref[...].astype(jnp.float32)
-        for tap in range(tap_count):
-            taps[8 * tap : 8 * tap + 8, :] = jnp.broadcast_to(kernel[tap : tap + 1, :], (8, lanes))
-
-    @pl.when(at_tile == 0)
-    def _():
-        rows[0:32, :] = rim_ref[...].astype(jnp.float32)
-
-    @pl.when(at_tile > 0)
-    def _():
-        rows[0:32, :] = gated(value_halo_ref, gate_halo_ref)
-
-    rows[32:, :] = gated(value_ref, gate_ref)
+    kernel = kernel_ref[...].astype(jnp.float32)
+    for tap in range(tap_count):
+        taps[8 * tap : 8 * tap + 8, :] = jnp.broadcast_to(kernel[tap : tap + 1, :], (8, lanes))
+    rim_ids = rim_ref[32:64, :].astype(jnp.float32)
+    rim_row = lax.broadcasted_iota(jnp.int32, rim_ids.shape, 0)
+    rim_first = jnp.max(jnp.where(rim_row == 2, rim_ids, jnp.float32(0.0))).astype(jnp.int32)
+
+    def begins(doc):
+        own = jnp.sum(jnp.where(ids_grid_ref[...] < doc, jnp.float32(1.0), jnp.float32(0.0)))
+        earlier = jnp.logical_and(rim_row >= 2, rim_ids < doc.astype(jnp.float32))
+        before = jnp.sum(jnp.where(earlier, jnp.float32(1.0), jnp.float32(0.0)))
+        return (own + before * jnp.float32(1.0 / lanes)).astype(jnp.int32)
 
     def convolve(source, at):
         acc = jnp.zeros((CHUNK // 8, 8, lanes), jnp.float32)
@@ -68,112 +44,98 @@
             acc = acc + window * taps[8 * tap : 8 * tap + 8, :][None]
         return acc.reshape(CHUNK, lanes)
 
-    base = at_tile * tile
-    low, high = edge_ref[0, at_tile], edge_ref[1, at_tile]
-    whole = jnp.logical_and(low == high, starts_ref[low] <= base)
-
-    @pl.when(whole)
-    def _():
+    def one_tile(step, carry):
+        at_tile = step ^ place_ref[0]
+        base = pl.multiple_of(at_tile * tile, tile)
+        rows[32:, :] = gated_ref[pl.ds(base, tile), :].astype(jnp.float32)
+
+        @pl.when(at_tile == 0)
+        def _():
+            rows[0:32, :] = rim_ref[0:32, :].astype(jnp.float32)
+
+        @pl.when(at_tile > 0)
+        def _():
+            halo = pl.ds(pl.multiple_of(jnp.maximum(base - 32, 0), 32), 32)
+            rows[0:32, :] = gated_ref[halo, :].astype(jnp.float32)
+
+        def oldest(at):
+            reach = base + at - 30
+            return jnp.where(reach < 0, rim_first, ids_ref[jnp.maximum(reach, 0)])
+
         for at in range(0, tile, CHUNK):
-            total[at : at + CHUNK, :] = convolve(rows, at)
-
-    @pl.when(jnp.logical_not(whole))
-    def _():
-        total[...] = jnp.zeros_like(total)
-
-        def one_document(doc, carry):
-            first = starts_ref[doc] - base + 2
-            last = starts_ref[doc + 1] - base + 2
-            position = lax.broadcasted_iota(jnp.int32, rows.shape, 0)
-            masked[...] = jnp.where(
-                jnp.logical_and(position >= first, position < last), rows[...], jnp.float32(0.0)
-            )
-            for at in range(0, tile, CHUNK):
-                place = lax.broadcasted_iota(jnp.int32, (CHUNK, lanes), 0) + (at + 32)
-                inside = jnp.logical_and(place >= first, place < last)
-                total[at : at + CHUNK, :] += jnp.where(
-                    inside, convolve(masked, at), jnp.float32(0.0)
-                )
+
+            @pl.when(oldest(at) == ids_ref[base + at + CHUNK - 1])
+            def _(at=at):
+                total[at : at + CHUNK, :] = convolve(rows, at)
+
+        def one_chunk(chunk, carry):
+            at = pl.multiple_of(chunk * CHUNK, CHUNK)
+            low, high = ids_ref[base + at], ids_ref[base + at + CHUNK - 1]
+
+            @pl.when(oldest(at) != high)
+            def _():
+                total[pl.ds(at, CHUNK), :] = jnp.zeros((CHUNK, lanes), jnp.float32)
+
+                def one_document(doc, carry):
+                    first = begins(doc) - base - at + 2
+                    last = begins(doc + 1) - base - at + 2
+                    position = lax.broadcasted_iota(jnp.int32, masked.shape, 0)
+                    masked[...] = jnp.where(
+                        jnp.logical_and(position >= first, position < last),
+                        rows[pl.ds(at, CHUNK + 32), :],
+                        jnp.float32(0.0),
+                    )
+                    place = lax.broadcasted_iota(jnp.int32, (CHUNK, lanes), 0) + 32
+                    inside = jnp.logical_and(place >= first, place < last)
+                    total[pl.ds(at, CHUNK), :] += jnp.where(
+                        inside, convolve(masked, 0), jnp.float32(0.0)
+                    )
+                    return carry
+
+                lax.fori_loop(low, high + 1, one_document, 0)
+
             return carry
 
-        lax.fori_loop(low, high + 1, one_document, 0)
-
-    for slot, out in enumerate(outs):
-
-        @pl.when(step == slot)
-        def _(out=out):
-            out[...] = total[...].astype(out.dtype)
-
-
-def convolve_tokens(place, starts, edges, value, gate, rim, kernel, parts):
-    tokens, lanes = value.shape
+        lax.fori_loop(0, tile // CHUNK, one_chunk, 0)
+        for slot, out in enumerate(outs):
+
+            @pl.when(step == slot)
+            def _(out=out):
+                out[...] = total[...].astype(out.dtype)
+
+        return carry
+
+    lax.fori_loop(0, len(outs), one_tile, 0)
+
+
+def convolve_tokens(place, ids, gated, rim, kernel, parts):
+    tokens, lanes = gated.shape
     taps = kernel.shape[0]
     tile = tokens // parts
-
-    def here(i, place, *_):
-        return (i ^ place[0], 0)
-
-    def halo(i, place, *_):
-        return (jnp.maximum((i ^ place[0]) * (tile // 32) - 1, 0), 0)
-
-    def whole(i, *_):
-        return (0, 0)
-
     return pl.pallas_call(
         conv_kernel_body,
-        grid_spec=pltpu.PrefetchScalarGridSpec(
-            num_scalar_prefetch=3,
-            grid=(parts,),
-            in_specs=[
-                pl.BlockSpec((tile, lanes), here),
-                pl.BlockSpec((tile, lanes), here),
-                pl.BlockSpec((32, lanes), halo),
-                pl.BlockSpec((32, lanes), halo),
-                pl.BlockSpec((32, lanes), whole),
-                pl.BlockSpec((taps, lanes), whole),
-            ],
-            out_specs=[pl.BlockSpec((tile, lanes), whole)] * parts,
-            scratch_shapes=[
-                pltpu.VMEM((8 * taps, lanes), jnp.float32),
-                pltpu.VMEM((tile + 32, lanes), jnp.float32),
-                pltpu.VMEM((tile + 32, lanes), jnp.float32),
-                pltpu.VMEM((tile, lanes), jnp.float32),
-            ],
-        ),
+        in_specs=[SMEM] * 2 + [VMEM] * 4,
+        out_specs=[VMEM] * parts,
+        scratch_shapes=[
+            pltpu.VMEM((8 * taps, lanes), jnp.float32),
+            pltpu.VMEM((tile + 32, lanes), jnp.float32),
+            pltpu.VMEM((CHUNK + 32, lanes), jnp.float32),
+            pltpu.VMEM((tile, lanes), jnp.float32),
+        ],
         out_shape=[jax.ShapeDtypeStruct((tile, lanes), jnp.bfloat16)] * parts,
         compiler_params=params(12),
         name="gated_conv",
-    )(place, starts, edges, value, gate, value, gate, rim, kernel)
-
-
-def rim_body(value_ref, gate_ref, ids_ref, out_ref):
-    tokens, lanes = value_ref.shape
-    tail = slice(tokens - 32, tokens)
-    out_ref[0:32, :] = (
-        value_ref[tail, :].astype(jnp.float32)
-        * jax.nn.sigmoid(gate_ref[tail, :].astype(jnp.float32))
-    ).astype(jnp.bfloat16)
-    row = lax.broadcasted_iota(jnp.int32, (32, lanes), 0)
-    ids = jnp.zeros((32, lanes), jnp.int32)
-    for place in range(32):
-        ids = jnp.where(row == place, ids_ref[tokens - 32 + place], ids)
-    out_ref[32:64, :] = ids.astype(jnp.float32).astype(jnp.bfloat16)
-
-
-def slots_body(capacity, place_ref, routing_ref, spread_ref, first_ref, second_ref, choice_ref):
+    )(place, ids, ids.reshape(-1, 128), gated, rim, kernel)
+
+
+def slots_body(capacity, routing_ref, spread_ref, first_ref, second_ref, choice_ref):
     count = routing_ref.shape[1]
     slots = spread_ref.shape[0]
     row = lax.broadcasted_iota(jnp.int32, (count, count), 0)
     column = lax.broadcasted_iota(jnp.int32, (count, count), 1)
-    role, device = place_ref[5], place_ref[4]
 
     def ones(mask):
         return jnp.where(mask, jnp.float32(1.0), jnp.float32(0.0))
-
-    def slot_of(expert, position):
-        apart = expert ^ device
-        swapped = (apart & 3) * 4 + (apart >> 2)
-        return jnp.where(role == 0, swapped, apart) * capacity + position.astype(jnp.int32)
 
     sub = lax.broadcasted_iota(jnp.int32, (16, count), 0)
     one, two = routing_ref[0:1, :], routing_ref[1:2, :]
@@ -187,7 +149,7 @@
     targets = []
     for chosen in (one, two):
         position = jnp.sum(jnp.where(sub == chosen, before, 0.0), axis=0, keepdims=True)
-        targets.append(slot_of(chosen, position))
+        targets.append(chosen * capacity + position.astype(jnp.int32))
     spread_ref[...] = ones(jnp.logical_or(slot == targets[0], slot == targets[1])).astype(
         jnp.bfloat16
     )
@@ -309,7 +271,7 @@
     spread_ref,
     state_ref,
     mix_ref,
-    *outgoing_refs,
+    outgoing_ref,
 ):
     projected = (
         residual_ref[...].astype(jnp.float32) + mine_ref[...] + other_ref[...].astype(jnp.float32)
@@ -319,10 +281,9 @@
     state = state.astype(jnp.float32)
     power = jnp.mean(state * state, axis=1, keepdims=True)
     normed = (state * lax.rsqrt(power + epsilon) * gain_moe_ref[...]).astype(jnp.bfloat16)
-    outgoing = jnp.dot(spread_ref[...], normed, preferred_element_type=jnp.float32)
-    block = outgoing_refs[0].shape[0]
-    for number, ref in enumerate(outgoing_refs):
-        ref[...] = outgoing[number * block : number * block + block].astype(jnp.bfloat16)
+    outgoing_ref[...] = jnp.dot(
+        spread_ref[...], normed, preferred_element_type=jnp.float32
+    ).astype(jnp.bfloat16)
     logits = lax.dot_general(
         normed, router_ref[...], (((1,), (1,)), ((), ())), preferred_element_type=jnp.float32
     )
@@ -354,9 +315,8 @@
     )
 
 
-def mix_body(state_ref, first_ref, second_ref, mix_ref, *refs):
-    returned_refs, out_ref = refs[:-1], refs[-1]
-    returned = jnp.concatenate([returned[...] for returned in returned_refs], axis=0)
+def mix_body(state_ref, first_ref, second_ref, mix_ref, returned_ref, out_ref):
+    returned = returned_ref[...]
     first = jnp.dot(first_ref[...], returned, preferred_element_type=jnp.float32)
     second = jnp.dot(second_ref[...], returned, preferred_element_type=jnp.float32)
     mixture = mix_ref[:, 0:1] * first + mix_ref[:, 1:2] * second
@@ -370,18 +330,6 @@
 
 def cross(array, by, turn):
     pairs = [(i, i ^ (by * (16 if (i & 1) == turn else 64))) for i in range(256)]
-    return lax.ppermute(array, ("sp", "tp"), pairs)
-
-
-def role_of(core, y, x):
-    return core ^ (x & 1) ^ (y & 1)
-
-
-def deal(array, by, turn):
-    pairs = []
-    for i in range(256):
-        along_x = role_of(i & 1, i >> 6, i >> 4 & 3) == turn
-        pairs.append((i, i ^ (by * (16 if along_x else 64)) ^ (by & 1)))
     return lax.ppermute(array, ("sp", "tp"), pairs)
 
 
@@ -409,7 +357,6 @@
     expert_down_w,
 ):
     tokens, lanes = conv_value.shape
-    rim = conv_kernel.shape[0] - 1
     count, width = residual.shape
     groups, experts = group_router.shape[1], expert_router.shape[1]
     slots = 2 * count
@@ -418,17 +365,15 @@
     sp, tp = lax.axis_index("sp"), lax.axis_index("tp")
     z, core, y, x = tp >> 1, tp & 1, sp >> 2, sp & 3
     u, v = jnp.where(core == 0, x, y), jnp.where(core == 0, y, x)
-    place = jnp.stack([z, core, v, u, sp, role_of(core, y, x)]).astype(jnp.int32)
+    place = jnp.stack([z, core, v, u]).astype(jnp.int32)
     depth = proj_weight.shape[0]
 
-    message = pl.pallas_call(
-        rim_body,
-        in_specs=[VMEM, VMEM, SMEM],
-        out_specs=VMEM,
-        out_shape=jax.ShapeDtypeStruct((64, lanes), jnp.bfloat16),
-        compiler_params=params(8),
-        name="tail",
-    )(conv_value, conv_gate, doc_ids)
+    gated = (
+        conv_value.astype(jnp.float32) * jax.nn.sigmoid(conv_gate.astype(jnp.float32))
+    ).astype(jnp.bfloat16)
+    tail = slice(tokens - 32, tokens)
+    tail_ids = jnp.broadcast_to(doc_ids[tail][:, None], (32, lanes)).astype(jnp.bfloat16)
+    message = jnp.concatenate([gated[tail], tail_ids], axis=0)
     came = shifted(message, "sp", 1)
 
     held = lax.dynamic_slice_in_dim(proj_weight, (v * 4 + u) * 128, 128, axis=1)[None]
@@ -445,22 +390,14 @@
     high_12 = cross(jnp.stack([high, high_3]), 1, 1)
     pieces = [low, low_1, low_32, high, high_3, high_12]
 
-    rim_values, rim_ids = came[:32], came[64 - rim :, 0].astype(jnp.int32)
-    padded_ids = jnp.concatenate([rim_ids, doc_ids], axis=0)
-    bounds = jnp.arange(24, dtype=jnp.int32)
-    starts = jnp.sum((padded_ids[None, :] < bounds[:, None]).astype(jnp.int32), axis=1)
-    tiles = doc_ids.reshape(8, tokens // 8)
-    edges = jnp.stack([tiles[:, 0], tiles[:, -1]])
-    convolved = convolve_tokens(
-        place, starts, edges, conv_value, conv_gate, rim_values, conv_kernel, 8
-    )
+    convolved = convolve_tokens(place, doc_ids, gated, came, conv_kernel, 8)
     raw = []
     for d in ORDER:
         raw.append(swap(convolved[d], dz=d) if d else convolved[d])
 
     spread, first_pick, second_pick, choice = pl.pallas_call(
         functools.partial(slots_body, capacity),
-        in_specs=[SMEM, VMEM],
+        in_specs=[VMEM],
         out_specs=[VMEM] * 4,
         out_shape=[
             jax.ShapeDtypeStruct((slots, count), jnp.bfloat16),
@@ -470,7 +407,7 @@
         ],
         compiler_params=params(8),
         name="slots",
-    )(place, routing.T)
+    )(routing.T)
     routers = jnp.concatenate(
         [
             expert_router.T,
@@ -519,16 +456,15 @@
         compiler_params=params(24),
         name="partial",
     )(place, active, *pieces)
-    block = slots // 4
-    state, mix, *outgoing = pl.pallas_call(
+    state, mix, outgoing = pl.pallas_call(
         functools.partial(state_body, groups, experts),
         in_specs=[VMEM] * 7,
-        out_specs=[VMEM] * 6,
+        out_specs=[VMEM] * 3,
         out_shape=[
             jax.ShapeDtypeStruct((count, width), jnp.bfloat16),
             jax.ShapeDtypeStruct((count, 32), jnp.float32),
-        ]
-        + [jax.ShapeDtypeStruct((block, width), jnp.bfloat16)] * 4,
+            jax.ShapeDtypeStruct((slots, width), jnp.bfloat16),
+        ],
         compiler_params=params(24),
         name="state",
     )(
@@ -541,36 +477,28 @@
         spread,
     )
 
-    def regrouped(blocks, which):
-        return jnp.concatenate(
-            [blocks[i][which * capacity : which * capacity + capacity] for i in range(4)], axis=0
+    def exchanged(rows):
+        blocks = rows.reshape(experts, capacity, width)
+        return lax.all_to_all(blocks, "sp", split_axis=0, concat_axis=0, tiled=True).reshape(
+            slots, width
         )
 
-    passing = {0: outgoing[0]} | {d: deal(outgoing[d], d, 0) for d in NEAR[1:]}
-    arrived = {d: regrouped(passing, d) for d in NEAR}
-    arrived = {d: deal(arrived[d], d, 1) if d else arrived[d] for d in NEAR}
-    results = {
-        d: pl.pallas_call(
-            experts_body,
-            in_specs=[VMEM] * 4,
-            out_specs=VMEM,
-            out_shape=jax.ShapeDtypeStruct((block, width), jnp.bfloat16),
-            compiler_params=params(16),
-            name="experts",
-        )(arrived[d], expert_gate_w[0], expert_up_w[0], expert_down_w[0])
-        for d in NEAR
-    }
-    results = {d: deal(results[d], d, 1) if d else results[d] for d in NEAR}
-    returned = {d: regrouped(results, d) for d in NEAR}
-    returned = {d: deal(returned[d], d, 0) if d else returned[d] for d in NEAR}
+    result = pl.pallas_call(
+        experts_body,
+        in_specs=[VMEM] * 4,
+        out_specs=VMEM,
+        out_shape=jax.ShapeDtypeStruct((slots, width), jnp.bfloat16),
+        compiler_params=params(20),
+        name="experts",
+    )(exchanged(outgoing), expert_gate_w[0], expert_up_w[0], expert_down_w[0])
     return pl.pallas_call(
         mix_body,
-        in_specs=[VMEM] * 8,
+        in_specs=[VMEM] * 5,
         out_specs=VMEM,
         out_shape=jax.ShapeDtypeStruct((count, width), jnp.bfloat16),
         compiler_params=params(16),
         name="mix",
-    )(state, first_pick, second_pick, mix, *[returned[d] for d in range(4)])
+    )(state, first_pick, second_pick, mix, exchanged(result))
 
 
 def solution(mesh):

time: 155 us -> 160 us (1.032)
  the two profiles are of different devices: /device:TPU:1 before, /device:TPU:0 now
where the time goes in v1:
time: 160 us; the launch traced here: 158 us
  blocking collectives  57.3 us (36%)
  waiting for transfers between devices  38.7 us (24%)
  starting transfers between devices  38.6 us (24%)
  Pallas kernels  18.5 us (12%)
  other arithmetic  3.11 us (2%)
    all_to_all x2, blocking collectives, exchanged(): lax.all_to_all(blocks, 'sp', split_axis=0, concat_axis=0, tiled=True)  57.3 us
    ppermute x12, starting transfers between devices, swap(): lax.ppermute(array, ('sp', 'tp'), [(i, i ^ flip) for i in range(256)])  26.8 us
    ppermute x12, waiting for transfers between devices, swap(): lax.ppermute(array, ('sp', 'tp'), [(i, i ^ flip) for i in range(256)])  22.6 us
    ppermute x7, waiting for transfers between devices, cross(): return lax.ppermute(array, ('sp', 'tp'), pairs)  14.8 us
    ppermute x7, starting transfers between devices, cross(): return lax.ppermute(array, ('sp', 'tp'), pairs)  10 us
    pallas_call x1, Pallas kernels, convolve_tokens(): pl.pallas_call(conv_kernel_body, in_specs=[SMEM] * 2 + [VMEM] * 4, out_sp...  6.57 us
    pallas_call x1, Pallas kernels, body(): pl.pallas_call(partial_body, in_specs=[SMEM, VMEM] + [pl.BlockSpec(memory...  3.97 us
  transfers between devices with their start and end apart: 20, of which 15 were waited for; matrix products, arithmetic and copies ran while one was open for 2% of the time, Pallas kernels for 5%

profile of v1, /device:TPU:0, one launch (start us, length us, event | category | flops | bytes accessed | tf_op | source)
XLA Modules:
  0.0 157.8 jit_solution(670856576012150080)
XLA Ops:
  0.0 1.0 copy-done
  1.1 5.6 %collective-permute-start.9 = (bf16[1,128,128]{2,1,0:T(8,128)(2,1)S(1)}, bf16[1,128,128]{2,1,0:T(8,128)(2,1)S(1)}, u32[]{:S(2)}, u32[]{:S(2)}) collective-permute-start(bf16[1,128,128]{2,1,0:T(8,128)(2,1)S(1)} %dynamic-slice_bitcast_fusion), channel_id=1, source_target_pairs={{0,8},{1,9},{2,10},{3,11},{4,12},{5,13},{6,14},{7,15},{8,0},{9,1},... | collective-permute-start | bytes 98312 | tf_op jit(solution)/shard_map/ppermute | solution.py:328
  6.6 2.3 %collective-permute-done.9 = bf16[1,128,128]{2,1,0:T(8,128)(2,1)S(1)} collective-permute-done((bf16[1,128,128]{2,1,0:T(8,128)(2,1)S(1)}, bf16[1,128,128]{2,1,0:T(8,128)(2,1)S(1)}, u32[]{:S(2)}, u32[]{:S(2)}) %collective-permute-start.9) | collective-permute-done | bytes 32800 | tf_op jit(solution)/shard_map/ppermute | solution.py:328
  9.0 1.8 %collective-permute-start.10 = (bf16[2,128,128]{2,1,0:T(8,128)(2,1)S(1)}, bf16[2,128,128]{2,1,0:T(8,128)(2,1)S(1)}, u32[]{:S(2)}, u32[]{:S(2)}) collective-permute-start(bf16[2,128,128]{2,1,0:T(8,128)(2,1)S(1)} %pad_maximum_fusion.6), channel_id=1, source_target_pairs={{0,4},{1,5},{2,6},{3,7},{4,0},{5,1},{6,2},{7,3},{8,12},{9,13},{10,... | collective-permute-start | bytes 196616 | tf_op jit(solution)/shard_map/ppermute | solution.py:328
  10.7 4.2 %collective-permute-done.10 = bf16[2,128,128]{2,1,0:T(8,128)(2,1)S(1)} collective-permute-done((bf16[2,128,128]{2,1,0:T(8,128)(2,1)S(1)}, bf16[2,128,128]{2,1,0:T(8,128)(2,1)S(1)}, u32[]{:S(2)}, u32[]{:S(2)}) %collective-permute-start.10) | collective-permute-done | bytes 65568 | tf_op jit(solution)/shard_map/ppermute | solution.py:328
  15.0 0.1 collective-permute-start.11
  15.1 5.0 %collective-permute-done.11 = bf16[4,128,128]{2,1,0:T(8,128)(2,1)S(1)} collective-permute-done((bf16[4,128,128]{2,1,0:T(8,128)(2,1)S(1)}, bf16[4,128,128]{2,1,0:T(8,128)(2,1)S(1)}, u32[]{:S(2)}, u32[]{:S(2)}) %collective-permute-start.11) | collective-permute-done | bytes 131104 | tf_op jit(solution)/shard_map/ppermute | solution.py:328
  20.0 1.1 collective-permute-start.12
  21.2 2.1 %collective-permute-start.13 = (bf16[8,128,128]{2,1,0:T(8,128)(2,1)S(1)}, bf16[8,128,128]{2,1,0:T(8,128)(2,1)S(1)}, u32[]{:S(2)}, u32[]{:S(2)}) collective-permute-start(bf16[8,128,128]{2,1,0:T(8,128)(2,1)S(1)} %pad_maximum_fusion.4), channel_id=1, source_target_pairs={{0,48},{1,193},{2,50},{3,195},{4,52},{5,197},{6,54},{7,199},{8,56}... | collective-permute-start | bytes 786440 | tf_op jit(solution)/shard_map/ppermute | solution.py:333
  23.3 1.0 collective-permute-start.14
  24.2 2.3 %collective-permute-done.12 = bf16[8,128,128]{2,1,0:T(8,128)(2,1)S(1)} collective-permute-done((bf16[8,128,128]{2,1,0:T(8,128)(2,1)S(1)}, bf16[8,128,128]{2,1,0:T(8,128)(2,1)S(1)}, u32[]{:S(2)}, u32[]{:S(2)}) %collective-permute-start.12) | collective-permute-done | bytes 262176 | tf_op jit(solution)/shard_map/ppermute | solution.py:333
  26.5 5.4 %collective-permute-done.13 = bf16[8,128,128]{2,1,0:T(8,128)(2,1)S(1)} collective-permute-done((bf16[8,128,128]{2,1,0:T(8,128)(2,1)S(1)}, bf16[8,128,128]{2,1,0:T(8,128)(2,1)S(1)}, u32[]{:S(2)}, u32[]{:S(2)}) %collective-permute-start.13) | collective-permute-done | bytes 262176 | tf_op jit(solution)/shard_map/ppermute | solution.py:333
  32.1 3.1 %collective-permute-start.17 = (bf16[4,4,128,128]{3,2,1,0:T(8,128)(2,1)S(1)}, bf16[4,4,128,128]{3,2,1,0:T(8,128)(2,1)S(1)}, u32[]{:S(2)}, u32[]{:S(2)}) collective-permute-start(bf16[4,4,128,128]{3,2,1,0:T(8,128)(2,1)S(1)} %get-tuple-element.40.high_ref), channel_id=1, source_target_pairs={{0,192},{1,49},{2,194},{3,51},{4,196},{5,53},{6,198},{7,55},{8,200... | collective-permute-start | bytes 1572872 | tf_op jit(solution)/shard_map/ppermute | solution.py:333
  35.3 0.2 collective-permute-start.15
  35.5 0.4 multiply_convert_fusion.gated_ref
  35.9 6.6 %collective-permute-done.17.high_3_ref = bf16[4,4,128,128]{3,2,1,0:T(8,128)(2,1)S(1)} collective-permute-done((bf16[4,4,128,128]{3,2,1,0:T(8,128)(2,1)S(1)}, bf16[4,4,128,128]{3,2,1,0:T(8,128)(2,1)S(1)}, u32[]{:S(2)}, u32[]{:S(2)}) %collective-permute-start.17) | collective-permute-done | bytes 524320 | tf_op jit(solution)/shard_map/ppermute | solution.py:333
  42.5 1.1 pad_maximum_fusion.1
  43.6 0.4 collective-permute-start.18
  44.0 0.5 collective-permute-done.15.low_1_ref
  44.5 1.1 pad_maximum_fusion
  45.6 2.1 %collective-permute-start.16 = (bf16[2,4,4,128,128]{4,3,2,1,0:T(8,128)(2,1)}, bf16[2,4,4,128,128]{4,3,2,1,0:T(8,128)(2,1)}, u32[]{:S(2)}, u32[]{:S(2)}) collective-permute-start(bf16[2,4,4,128,128]{4,3,2,1,0:T(8,128)(2,1)} %pad_maximum_fusion), channel_id=1, source_target_pairs={{0,192},{1,49},{2,194},{3,51},{4,196},{5,53},{6,198},{7,55},{8,200... | collective-permute-start | bytes 3145736 | tf_op jit(solution)/shard_map/ppermute | solution.py:333
  48.0 1.8 %collective-permute-start = (bf16[64,128]{1,0:T(8,128)(2,1)S(1)}, bf16[64,128]{1,0:T(8,128)(2,1)S(1)}, u32[]{:S(2)}, u32[]{:S(2)}) collective-permute-start(bf16[64,128]{1,0:T(8,128)(2,1)S(1)} %pad_maximum_fusion.7), channel_id=1, source_target_pairs={{0,16},{16,32},{32,48},{48,64},{64,80},{80,96},{96,112},{112,128},... | collective-permute-start | bytes 49160 | tf_op jit(solution)/shard_map/ppermute | solution.py:339
  49.9 1.3 collective-permute-done.rim_ref
  51.2 6.6 %gated_conv.1 = (bf16[384,128]{1,0:T(8,128)(2,1)S(1)}, bf16[384,128]{1,0:T(8,128)(2,1)S(1)}, bf16[384,128]{1,0:T(8,128)(2,1)S(1)}, bf16[384,128]{1,0:T(8,128)(2,...) custom-call(s32[4]{0:T(128)S(1)} %pad_add_fusion.place_ref, ...), custom_call_target="tpu_custom_call" | custom-call | tf_op jit(solution)/shard_map/gated_conv/pallas_call | solution.py:115
  57.8 5.3 %collective-permute-start.1 = (bf16[384,128]{1,0:T(8,128)(2,1)S(1)}, bf16[384,128]{1,0:T(8,128)(2,1)S(1)}, u32[]{:S(2)}, u32[]{:S(2)}) collective-permute-start(bf16[384,128]{1,0:T(8,128)(2,1)S(1)} %get-tuple-element.23), channel_id=1, source_target_pairs={{0,8},{1,9},{2,10},{3,11},{4,12},{5,13},{6,14},{7,15},{8,0},{9,1},... | collective-permute-start | bytes 294920 | tf_op jit(solution)/shard_map/ppermute | solution.py:328
  63.1 2.0 %collective-permute-start.2 = (bf16[384,128]{1,0:T(8,128)(2,1)S(1)}, bf16[384,128]{1,0:T(8,128)(2,1)S(1)}, u32[]{:S(2)}, u32[]{:S(2)}) collective-permute-start(bf16[384,128]{1,0:T(8,128)(2,1)S(1)} %get-tuple-element.24), channel_id=1, source_target_pairs={{0,4},{1,5},{2,6},{3,7},{4,0},{5,1},{6,2},{7,3},{8,12},{9,13},{10,... | collective-permute-start | bytes 294920 | tf_op jit(solution)/shard_map/ppermute | solution.py:328
  65.1 2.2 %collective-permute-done.1.refs_1_ = bf16[384,128]{1,0:T(8,128)(2,1)S(1)} collective-permute-done((bf16[384,128]{1,0:T(8,128)(2,1)S(1)}, bf16[384,128]{1,0:T(8,128)(2,1)S(1)}, u32[]{:S(2)}, u32[]{:S(2)}) %collective-permute-start.1) | collective-permute-done | bytes 98336 | tf_op jit(solution)/shard_map/ppermute | solution.py:328
  67.2 4.1 %collective-permute-start.4 = (bf16[384,128]{1,0:T(8,128)(2,1)S(1)}, bf16[384,128]{1,0:T(8,128)(2,1)S(1)}, u32[]{:S(2)}, u32[]{:S(2)}) collective-permute-start(bf16[384,128]{1,0:T(8,128)(2,1)S(1)} %get-tuple-element.26), channel_id=1, source_target_pairs={{0,2},{1,3},{2,0},{3,1},{4,6},{5,7},{6,4},{7,5},{8,10},{9,11},{10,... | collective-permute-start | bytes 294920 | tf_op jit(solution)/shard_map/ppermute | solution.py:328
  71.3 0.7 collective-permute-done.2.refs_2_
  72.0 4.7 %collective-permute-start.5 = (bf16[384,128]{1,0:T(8,128)(2,1)S(1)}, bf16[384,128]{1,0:T(8,128)(2,1)S(1)}, u32[]{:S(2)}, u32[]{:S(2)}) collective-permute-start(bf16[384,128]{1,0:T(8,128)(2,1)S(1)} %get-tuple-element.27), channel_id=1, source_target_pairs={{0,10},{1,11},{2,8},{3,9},{4,14},{5,15},{6,12},{7,13},{8,2},{9,3},... | collective-permute-start | bytes 294920 | tf_op jit(solution)/shard_map/ppermute | solution.py:328
  76.8 1.0 collective-permute-start.6
  77.8 1.8 %collective-permute-start.7 = (bf16[384,128]{1,0:T(8,128)(2,1)S(1)}, bf16[384,128]{1,0:T(8,128)(2,1)S(1)}, u32[]{:S(2)}, u32[]{:S(2)}) collective-permute-start(bf16[384,128]{1,0:T(8,128)(2,1)S(1)} %get-tuple-element.29), channel_id=1, source_target_pairs={{0,14},{1,15},{2,12},{3,13},{4,10},{5,11},{6,8},{7,9},{8,6},{9,7},... | collective-permute-start | bytes 294920 | tf_op jit(solution)/shard_map/ppermute | solution.py:328
  79.5 2.2 %collective-permute-done.5.refs_5_ = bf16[384,128]{1,0:T(8,128)(2,1)S(1)} collective-permute-done((bf16[384,128]{1,0:T(8,128)(2,1)S(1)}, bf16[384,128]{1,0:T(8,128)(2,1)S(1)}, u32[]{:S(2)}, u32[]{:S(2)}) %collective-permute-start.5) | collective-permute-done | bytes 98336 | tf_op jit(solution)/shard_map/ppermute | solution.py:328
  81.8 1.5 collective-permute-done.6.refs_6_
  83.3 1.5 collective-permute-done.7.refs_7_
  84.8 0.4 stats.1.mine_ref
  85.2 0.3 collective-permute-start.8
  85.5 1.4 collective-permute-done.8.other_ref
  86.9 1.2 activate.1.active_ref
  88.2 4.0 %partial.1 = (f32[192,2048]{1,0:T(8,128)S(1)}, bf16[192,2048]{1,0:T(8,128)(2,1)S(1)}) custom-call(s32[4]{0:T(128)S(1)} %pad_add_fusion.place_ref, bf16[384,1024]{1,0:T(8,128)(2,1)S(1)} %activate.1.active_ref, bf16[4,4,128,128]{3,2,1,0:T(8,128)(2,1)S(1)} %get-tuple-element.42.low_ref, bf16[4,4,128,128]{3,2,1,0:T(8,128)(2,1)S(1)} %collective-permute-done.15.low_1_ref, ...), custom_call_target="tpu_custom_call" | custom-call | tf_op jit(solution)/shard_map/partial/pallas_call | solution.py:444
  92.1 0.2 collective-permute-start.19
  92.4 0.4 slots.1
  93.0 1.6 collective-permute-done.19.other_ref
  94.5 1.4 state.1
  95.9 32.0 %all_to_all.10 = bf16[16,24,2048]{2,1,0:T(8,128)(2,1)S(1)} all-to-all(bf16[16,24,2048]{2,1,0:T(8,128)(2,1)S(1)} %bitcast.49), channel_id=1, replica_groups=mesh['sp'=16,'tp'=16] {'sp'}, dimensions={0} | all-to-all | bytes 3145728 | tf_op jit(solution)/shard_map/all_to_all | solution.py:482
  128.0 2.6 %experts.1 = bf16[384,2048]{1,0:T(8,128)(2,1)S(1)} custom-call(bf16[384,2048]{1,0:T(8,128)(2,1)S(1)} %bitcast.42, bf16[2048,512]{1,0:T(8,128)(2,1)S(1)} %bitcast.46, bf16[2048,512]{1,0:T(8,128)(2,1)S(1)} %bitcast.47, bf16[512,2048]{1,0:T(8,128)(2,1)S(1)} %bitcast.48), custom_call_target="tpu_custom_call" | custom-call | tf_op jit(solution)/shard_map/experts/pallas_call | solution.py:486
  130.6 25.2 %all_to_all.11 = bf16[16,24,2048]{2,1,0:T(8,128)(2,1)S(1)} all-to-all(bf16[16,24,2048]{2,1,0:T(8,128)(2,1)S(1)} %bitcast.43), channel_id=1, replica_groups=mesh['sp'=16,'tp'=16] {'sp'}, dimensions={0} | all-to-all | bytes 3145728 | tf_op jit(solution)/shard_map/all_to_all | solution.py:482
  155.8 1.9 %mix.1 = bf16[192,2048]{1,0:T(8,128)(2,1)} custom-call(bf16[192,2048]{1,0:T(8,128)(2,1)S(1)} %get-tuple-element.34.state_ref, bf16[192,384]{1,0:T(8,128)(2,1)S(1)} %get-tuple-element.35.first_ref, bf16[192,384]{1,0:T(8,128)(2,1)S(1)} %get-tuple-element.36.second_ref, f32[192,32]{1,0:T(8,128)S(1)} %get-tuple-element.37.mix_ref, bf16[384,2048]{1,0:T(8,128)(2,1)S(1)} %bitcast.41), custom_call_target="tpu_custom_call" | custom-call | tf_op jit(solution)/shard_map/mix/pallas_call | solution.py:494
  (52 shorter events, 0.9 us)
Async XLA Ops:
  0.0 1.0 copy-start
  1.1 7.9 %collective-permute-start.9 = (bf16[1,128,128]{2,1,0:T(8,128)(2,1)S(1)}, bf16[1,128,128]{2,1,0:T(8,128)(2,1)S(1)}, u32[]{:S(2)}, u32[]{:S(2)}) collective-permute-start(bf16[1,128,128]{2,1,0:T(8,128)(2,1)S(1)} %dynamic-slice_bitcast_fusion), channel_id=1, source_target_pairs={{0,8},{1,9},{2,10},{3,11},{4,12},{5,13},{6,14},{7,15},{8,0},{9,1},... | collective-permute-start | bytes 98312 | tf_op jit(solution)/shard_map/ppermute | solution.py:328
  9.0 6.0 %collective-permute-start.10 = (bf16[2,128,128]{2,1,0:T(8,128)(2,1)S(1)}, bf16[2,128,128]{2,1,0:T(8,128)(2,1)S(1)}, u32[]{:S(2)}, u32[]{:S(2)}) collective-permute-start(bf16[2,128,128]{2,1,0:T(8,128)(2,1)S(1)} %pad_maximum_fusion.6), channel_id=1, source_target_pairs={{0,4},{1,5},{2,6},{3,7},{4,0},{5,1},{6,2},{7,3},{8,12},{9,13},{10,... | collective-permute-start | bytes 196616 | tf_op jit(solution)/shard_map/ppermute | solution.py:328
  15.0 5.1 %collective-permute-start.11 = (bf16[4,128,128]{2,1,0:T(8,128)(2,1)S(1)}, bf16[4,128,128]{2,1,0:T(8,128)(2,1)S(1)}, u32[]{:S(2)}, u32[]{:S(2)}) collective-permute-start(bf16[4,128,128]{2,1,0:T(8,128)(2,1)S(1)} %get-tuple-element.50), channel_id=1, source_target_pairs={{0,2},{1,3},{2,0},{3,1},{4,6},{5,7},{6,4},{7,5},{8,10},{9,11},{10,... | collective-permute-start | bytes 393224 | tf_op jit(solution)/shard_map/ppermute | solution.py:328
  20.0 6.5 %collective-permute-start.12 = (bf16[8,128,128]{2,1,0:T(8,128)(2,1)S(1)}, bf16[8,128,128]{2,1,0:T(8,128)(2,1)S(1)}, u32[]{:S(2)}, u32[]{:S(2)}) collective-permute-start(bf16[8,128,128]{2,1,0:T(8,128)(2,1)S(1)} %pad_maximum_fusion.4), channel_id=1, source_target_pairs={{0,16},{1,65},{2,18},{3,67},{4,20},{5,69},{6,22},{7,71},{8,24},{9,... | collective-permute-start | bytes 786440 | tf_op jit(solution)/shard_map/ppermute | solution.py:333
  21.2 10.7 %collective-permute-start.13 = (bf16[8,128,128]{2,1,0:T(8,128)(2,1)S(1)}, bf16[8,128,128]{2,1,0:T(8,128)(2,1)S(1)}, u32[]{:S(2)}, u32[]{:S(2)}) collective-permute-start(bf16[8,128,128]{2,1,0:T(8,128)(2,1)S(1)} %pad_maximum_fusion.4), channel_id=1, source_target_pairs={{0,48},{1,193},{2,50},{3,195},{4,52},{5,197},{6,54},{7,199},{8,56}... | collective-permute-start | bytes 786440 | tf_op jit(solution)/shard_map/ppermute | solution.py:333
  23.3 8.6 %collective-permute-start.14 = (bf16[8,128,128]{2,1,0:T(8,128)(2,1)S(1)}, bf16[8,128,128]{2,1,0:T(8,128)(2,1)S(1)}, u32[]{:S(2)}, u32[]{:S(2)}) collective-permute-start(bf16[8,128,128]{2,1,0:T(8,128)(2,1)S(1)} %pad_maximum_fusion.4), channel_id=1, source_target_pairs={{0,32},{1,129},{2,34},{3,131},{4,36},{5,133},{6,38},{7,135},{8,40}... | collective-permute-start | bytes 786440 | tf_op jit(solution)/shard_map/ppermute | solution.py:333
  31.9 3.5 %copy-start.11 = (bf16[3072,128]{1,0:T(8,128)(2,1)S(1)}, bf16[3072,128]{1,0:T(8,128)(2,1)}, u32[]{:S(2)}) copy-start(bf16[3072,128]{1,0:T(8,128)(2,1)} %param.16) | copy-start | bytes 2359300
  32.0 3.5 %copy-start.12 = (bf16[3072,128]{1,0:T(8,128)(2,1)S(1)}, bf16[3072,128]{1,0:T(8,128)(2,1)}, u32[]{:S(2)}) copy-start(bf16[3072,128]{1,0:T(8,128)(2,1)} %param.15) | copy-start | bytes 2359300
  32.1 10.5 %collective-permute-start.17 = (bf16[4,4,128,128]{3,2,1,0:T(8,128)(2,1)S(1)}, bf16[4,4,128,128]{3,2,1,0:T(8,128)(2,1)S(1)}, u32[]{:S(2)}, u32[]{:S(2)}) collective-permute-start(bf16[4,4,128,128]{3,2,1,0:T(8,128)(2,1)S(1)} %get-tuple-element.40.high_ref), channel_id=1, source_target_pairs={{0,192},{1,49},{2,194},{3,51},{4,196},{5,53},{6,198},{7,55},{8,200... | collective-permute-start | bytes 1572872 | tf_op jit(solution)/shard_map/ppermute | solution.py:333
  35.3 9.3 %collective-permute-start.15 = (bf16[4,4,128,128]{3,2,1,0:T(8,128)(2,1)S(1)}, bf16[4,4,128,128]{3,2,1,0:T(8,128)(2,1)S(1)}, u32[]{:S(2)}, u32[]{:S(2)}) collective-permute-start(bf16[4,4,128,128]{3,2,1,0:T(8,128)(2,1)S(1)} %get-tuple-element.42.low_ref), channel_id=1, source_target_pairs={{0,64},{1,17},{2,66},{3,19},{4,68},{5,21},{6,70},{7,23},{8,72},{9,... | collective-permute-start | bytes 1572872 | tf_op jit(solution)/shard_map/ppermute | solution.py:333
  43.6 4.1 %copy-start.5 = (s32[3072]{0:T(1024)S(1)}, s32[3072]{0:T(1024)}, u32[]{:S(2)}) copy-start(s32[3072]{0:T(1024)} %ids_ref.1) | copy-start | bytes 36868
  43.6 7.6 %copy-start.6 = (bf16[31,128]{1,0:T(8,128)(2,1)S(1)}, bf16[31,128]{1,0:T(8,128)(2,1)}, u32[]{:S(2)}) copy-start(bf16[31,128]{1,0:T(8,128)(2,1)} %kernel_ref.1) | copy-start | bytes 23812
  43.6 44.5 %collective-permute-start.18 = (bf16[2,4,4,128,128]{4,3,2,1,0:T(8,128)(2,1)}, bf16[2,4,4,128,128]{4,3,2,1,0:T(8,128)(2,1)}, u32[]{:S(2)}, u32[]{:S(2)}) collective-permute-start(bf16[2,4,4,128,128]{4,3,2,1,0:T(8,128)(2,1)} %pad_maximum_fusion.1), channel_id=1, source_target_pairs={{0,64},{1,17},{2,66},{3,19},{4,68},{5,21},{6,70},{7,23},{8,72},{9,... | collective-permute-start | bytes 3145736 | tf_op jit(solution)/shard_map/ppermute | solution.py:333
  44.5 42.4 %copy-start.7 = (f32[2048]{0:T(1024)S(1)}, f32[2048]{0:T(1024)}, u32[]{:S(2)}) copy-start(f32[2048]{0:T(1024)} %param.19) | copy-start | bytes 24580
  44.5 42.4 %copy-start.8 = (f32[2048]{0:T(1024)S(1)}, f32[2048]{0:T(1024)}, u32[]{:S(2)}) copy-start(f32[2048]{0:T(1024)} %param.20) | copy-start | bytes 24580
  45.6 42.6 %collective-permute-start.16 = (bf16[2,4,4,128,128]{4,3,2,1,0:T(8,128)(2,1)}, bf16[2,4,4,128,128]{4,3,2,1,0:T(8,128)(2,1)}, u32[]{:S(2)}, u32[]{:S(2)}) collective-permute-start(bf16[2,4,4,128,128]{4,3,2,1,0:T(8,128)(2,1)} %pad_maximum_fusion), channel_id=1, source_target_pairs={{0,192},{1,49},{2,194},{3,51},{4,196},{5,53},{6,198},{7,55},{8,200... | collective-permute-start | bytes 3145736 | tf_op jit(solution)/shard_map/ppermute | solution.py:333
  48.0 3.2 %collective-permute-start = (bf16[64,128]{1,0:T(8,128)(2,1)S(1)}, bf16[64,128]{1,0:T(8,128)(2,1)S(1)}, u32[]{:S(2)}, u32[]{:S(2)}) collective-permute-start(bf16[64,128]{1,0:T(8,128)(2,1)S(1)} %pad_maximum_fusion.7), channel_id=1, source_target_pairs={{0,16},{16,32},{32,48},{48,64},{64,80},{80,96},{96,112},{112,128},... | collective-permute-start | bytes 49160 | tf_op jit(solution)/shard_map/ppermute | solution.py:339
  57.8 9.4 %collective-permute-start.1 = (bf16[384,128]{1,0:T(8,128)(2,1)S(1)}, bf16[384,128]{1,0:T(8,128)(2,1)S(1)}, u32[]{:S(2)}, u32[]{:S(2)}) collective-permute-start(bf16[384,128]{1,0:T(8,128)(2,1)S(1)} %get-tuple-element.23), channel_id=1, source_target_pairs={{0,8},{1,9},{2,10},{3,11},{4,12},{5,13},{6,14},{7,15},{8,0},{9,1},... | collective-permute-start | bytes 294920 | tf_op jit(solution)/shard_map/ppermute | solution.py:328
  63.1 8.9 %collective-permute-start.2 = (bf16[384,128]{1,0:T(8,128)(2,1)S(1)}, bf16[384,128]{1,0:T(8,128)(2,1)S(1)}, u32[]{:S(2)}, u32[]{:S(2)}) collective-permute-start(bf16[384,128]{1,0:T(8,128)(2,1)S(1)} %get-tuple-element.24), channel_id=1, source_target_pairs={{0,4},{1,5},{2,6},{3,7},{4,0},{5,1},{6,2},{7,3},{8,12},{9,13},{10,... | collective-permute-start | bytes 294920 | tf_op jit(solution)/shard_map/ppermute | solution.py:328
  65.1 11.7 %collective-permute-start.3 = (bf16[384,128]{1,0:T(8,128)(2,1)S(1)}, bf16[384,128]{1,0:T(8,128)(2,1)S(1)}, u32[]{:S(2)}, u32[]{:S(2)}) collective-permute-start(bf16[384,128]{1,0:T(8,128)(2,1)S(1)} %get-tuple-element.25), channel_id=1, source_target_pairs={{0,12},{1,13},{2,14},{3,15},{4,8},{5,9},{6,10},{7,11},{8,4},{9,5},... | collective-permute-start | bytes 294920 | tf_op jit(solution)/shard_map/ppermute | solution.py:328
  67.2 10.6 %collective-permute-start.4 = (bf16[384,128]{1,0:T(8,128)(2,1)S(1)}, bf16[384,128]{1,0:T(8,128)(2,1)S(1)}, u32[]{:S(2)}, u32[]{:S(2)}) collective-permute-start(bf16[384,128]{1,0:T(8,128)(2,1)S(1)} %get-tuple-element.26), channel_id=1, source_target_pairs={{0,2},{1,3},{2,0},{3,1},{4,6},{5,7},{6,4},{7,5},{8,10},{9,11},{10,... | collective-permute-start | bytes 294920 | tf_op jit(solution)/shard_map/ppermute | solution.py:328
  72.0 9.7 %collective-permute-start.5 = (bf16[384,128]{1,0:T(8,128)(2,1)S(1)}, bf16[384,128]{1,0:T(8,128)(2,1)S(1)}, u32[]{:S(2)}, u32[]{:S(2)}) collective-permute-start(bf16[384,128]{1,0:T(8,128)(2,1)S(1)} %get-tuple-element.27), channel_id=1, source_target_pairs={{0,10},{1,11},{2,8},{3,9},{4,14},{5,15},{6,12},{7,13},{8,2},{9,3},... | collective-permute-start | bytes 294920 | tf_op jit(solution)/shard_map/ppermute | solution.py:328
  76.8 6.5 %collective-permute-start.6 = (bf16[384,128]{1,0:T(8,128)(2,1)S(1)}, bf16[384,128]{1,0:T(8,128)(2,1)S(1)}, u32[]{:S(2)}, u32[]{:S(2)}) collective-permute-start(bf16[384,128]{1,0:T(8,128)(2,1)S(1)} %get-tuple-element.28), channel_id=1, source_target_pairs={{0,6},{1,7},{2,4},{3,5},{4,2},{5,3},{6,0},{7,1},{8,14},{9,15},{10,... | collective-permute-start | bytes 294920 | tf_op jit(solution)/shard_map/ppermute | solution.py:328
  77.8 7.0 %collective-permute-start.7 = (bf16[384,128]{1,0:T(8,128)(2,1)S(1)}, bf16[384,128]{1,0:T(8,128)(2,1)S(1)}, u32[]{:S(2)}, u32[]{:S(2)}) collective-permute-start(bf16[384,128]{1,0:T(8,128)(2,1)S(1)} %get-tuple-element.29), channel_id=1, source_target_pairs={{0,14},{1,15},{2,12},{3,13},{4,10},{5,11},{6,8},{7,9},{8,6},{9,7},... | collective-permute-start | bytes 294920 | tf_op jit(solution)/shard_map/ppermute | solution.py:328
  85.2 1.7 %collective-permute-start.8 = (f32[384,128]{1,0:T(8,128)S(1)}, f32[384,128]{1,0:T(8,128)S(1)}, u32[]{:S(2)}, u32[]{:S(2)}) collective-permute-start(f32[384,128]{1,0:T(8,128)S(1)} %stats.1.mine_ref), channel_id=1, source_target_pairs={{0,1},{1,0},{2,3},{3,2},{4,5},{5,4},{6,7},{7,6},{8,9},{9,8},{10,11... | collective-permute-start | bytes 589832 | tf_op jit(solution)/shard_map/ppermute | solution.py:328
  88.1 4.3 %copy-start.10 = (s32[192,2]{0,1:T(2,128)S(1)}, s32[192,2]{0,1:T(2,128)}, u32[]{:S(2)}) copy-start(s32[192,2]{0,1:T(2,128)} %param.26) | copy-start | bytes 4612
  88.1 4.8 %copy-start.13 = (bf16[2048,16]{0,1:T(8,128)(2,1)S(1)}, bf16[2048,16]{0,1:T(8,128)(2,1)}, u32[]{:S(2)}) copy-start(bf16[2048,16]{0,1:T(8,128)(2,1)} %param.25) | copy-start | bytes 196612
  88.1 4.8 %copy-start.14 = (bf16[2048,2]{0,1:T(2,128)(2,1)S(1)}, bf16[2048,2]{0,1:T(2,128)(2,1)}, u32[]{:S(2)}) copy-start(bf16[2048,2]{0,1:T(2,128)(2,1)} %param.24) | copy-start | bytes 24580
  88.1 6.4 %copy-start.4 = (bf16[192,2048]{1,0:T(8,128)(2,1)S(1)}, bf16[192,2048]{1,0:T(8,128)(2,1)}, u32[]{:S(2)}) copy-start(bf16[192,2048]{1,0:T(8,128)(2,1)} %residual_ref.1) | copy-start | bytes 2359300
  88.1 6.4 %copy-start.9 = (f32[2048]{0:T(1024)S(1)}, f32[2048]{0:T(1024)}, u32[]{:S(2)}) copy-start(f32[2048]{0:T(1024)} %param.23) | copy-start | bytes 24580
  92.1 2.4 %collective-permute-start.19 = (bf16[192,2048]{1,0:T(8,128)(2,1)S(1)}, bf16[192,2048]{1,0:T(8,128)(2,1)S(1)}, u32[]{:S(2)}, u32[]{:S(2)}) collective-permute-start(bf16[192,2048]{1,0:T(8,128)(2,1)S(1)} %get-tuple-element.31), channel_id=1, source_target_pairs={{0,1},{1,0},{2,3},{3,2},{4,5},{5,4},{6,7},{7,6},{8,9},{9,8},{10,11... | collective-permute-start | bytes 2359304 | tf_op jit(solution)/shard_map/ppermute | solution.py:328
  94.5 33.4 %copy-start.2 = (bf16[1,2048,512]{2,1,0:T(8,128)(2,1)S(1)}, bf16[1,2048,512]{2,1,0:T(8,128)(2,1)}, u32[]{:S(2)}) copy-start(bf16[1,2048,512]{2,1,0:T(8,128)(2,1)} %param.28) | copy-start | bytes 6291460
  94.5 33.4 %copy-start.3 = (bf16[1,512,2048]{2,1,0:T(8,128)(2,1)S(1)}, bf16[1,512,2048]{2,1,0:T(8,128)(2,1)}, u32[]{:S(2)}) copy-start(bf16[1,512,2048]{2,1,0:T(8,128)(2,1)} %param.29) | copy-start | bytes 6291460
  95.9 32.1 %copy-start.1 = (bf16[1,2048,512]{2,1,0:T(8,128)(2,1)S(1)}, bf16[1,2048,512]{2,1,0:T(8,128)(2,1)}, u32[]{:S(2)}) copy-start(bf16[1,2048,512]{2,1,0:T(8,128)(2,1)} %param.27) | copy-start | bytes 6291460

commit v2 on v1

--- a/solution.py
+++ b/solution.py
@@ -20,19 +20,22 @@
     return pltpu.CompilerParams(vmem_limit_bytes=mib * 1024 * 1024)
 
 
-def conv_kernel_body(place_ref, ids_ref, ids_grid_ref, gated_ref, rim_ref, kernel_ref, *refs):
-    outs, (taps, rows, masked, total) = refs[:-4], refs[-4:]
-    tile, lanes = outs[0].shape
+def conv_kernel_body(begin, ids_ref, ids_grid_ref, gated_ref, kernel_ref, *refs):
+    rims, (out_ref, taps, rows, masked, total) = refs[:-5], refs[-5:]
+    count, tile, lanes = out_ref.shape
     tap_count = kernel_ref.shape[0]
     kernel = kernel_ref[...].astype(jnp.float32)
     for tap in range(tap_count):
         taps[8 * tap : 8 * tap + 8, :] = jnp.broadcast_to(kernel[tap : tap + 1, :], (8, lanes))
-    rim_ids = rim_ref[32:64, :].astype(jnp.float32)
-    rim_row = lax.broadcasted_iota(jnp.int32, rim_ids.shape, 0)
-    rim_first = jnp.max(jnp.where(rim_row == 2, rim_ids, jnp.float32(0.0))).astype(jnp.int32)
+    rim_row = lax.broadcasted_iota(jnp.int32, (32, lanes), 0)
+    if begin == 0:
+        rim_ids = rims[0][32:64, :].astype(jnp.float32)
+        rim_first = jnp.max(jnp.where(rim_row == 2, rim_ids, jnp.float32(0.0))).astype(jnp.int32)
 
     def begins(doc):
         own = jnp.sum(jnp.where(ids_grid_ref[...] < doc, jnp.float32(1.0), jnp.float32(0.0)))
+        if begin > 0:
+            return own.astype(jnp.int32) + 30
         earlier = jnp.logical_and(rim_row >= 2, rim_ids < doc.astype(jnp.float32))
         before = jnp.sum(jnp.where(earlier, jnp.float32(1.0), jnp.float32(0.0)))
         return (own + before * jnp.float32(1.0 / lanes)).astype(jnp.int32)
@@ -45,21 +48,20 @@
         return acc.reshape(CHUNK, lanes)
 
     def one_tile(step, carry):
-        at_tile = step ^ place_ref[0]
-        base = pl.multiple_of(at_tile * tile, tile)
+        base = pl.multiple_of((begin + step) * tile, tile)
+        halo = pl.ds(pl.multiple_of(jnp.maximum(base - 32, 0), 32), 32)
         rows[32:, :] = gated_ref[pl.ds(base, tile), :].astype(jnp.float32)
-
-        @pl.when(at_tile == 0)
-        def _():
-            rows[0:32, :] = rim_ref[0:32, :].astype(jnp.float32)
-
-        @pl.when(at_tile > 0)
-        def _():
-            halo = pl.ds(pl.multiple_of(jnp.maximum(base - 32, 0), 32), 32)
-            rows[0:32, :] = gated_ref[halo, :].astype(jnp.float32)
+        rows[0:32, :] = gated_ref[halo, :].astype(jnp.float32)
+        if begin == 0:
+
+            @pl.when(step == 0)
+            def _():
+                rows[0:32, :] = rims[0][0:32, :].astype(jnp.float32)
 
         def oldest(at):
             reach = base + at - 30
+            if begin > 0:
+                return ids_ref[reach]
             return jnp.where(reach < 0, rim_first, ids_ref[jnp.maximum(reach, 0)])
 
         for at in range(0, tile, CHUNK):
@@ -97,35 +99,29 @@
             return carry
 
         lax.fori_loop(0, tile // CHUNK, one_chunk, 0)
-        for slot, out in enumerate(outs):
-
-            @pl.when(step == slot)
-            def _(out=out):
-                out[...] = total[...].astype(out.dtype)
-
+        out_ref[step] = total[...].astype(out_ref.dtype)
         return carry
 
-    lax.fori_loop(0, len(outs), one_tile, 0)
-
-
-def convolve_tokens(place, ids, gated, rim, kernel, parts):
-    tokens, lanes = gated.shape
+    lax.fori_loop(0, count, one_tile, 0)
+
+
+def convolve_tokens(begin, count, tile, ids, gated, kernel, *rims):
+    lanes = gated.shape[1]
     taps = kernel.shape[0]
-    tile = tokens // parts
     return pl.pallas_call(
-        conv_kernel_body,
-        in_specs=[SMEM] * 2 + [VMEM] * 4,
-        out_specs=[VMEM] * parts,
+        functools.partial(conv_kernel_body, begin),
+        in_specs=[SMEM] + [VMEM] * (3 + len(rims)),
+        out_specs=VMEM,
         scratch_shapes=[
             pltpu.VMEM((8 * taps, lanes), jnp.float32),
             pltpu.VMEM((tile + 32, lanes), jnp.float32),
             pltpu.VMEM((CHUNK + 32, lanes), jnp.float32),
             pltpu.VMEM((tile, lanes), jnp.float32),
         ],
-        out_shape=[jax.ShapeDtypeStruct((tile, lanes), jnp.bfloat16)] * parts,
+        out_shape=jax.ShapeDtypeStruct((count, tile, lanes), jnp.bfloat16),
         compiler_params=params(12),
-        name="gated_conv",
-    )(place, ids, ids.reshape(-1, 128), gated, rim, kernel)
+        name="conv_head" if begin == 0 else "conv_rest",
+    )(ids, ids.reshape(-1, 128), gated, kernel, *rims)
 
 
 def slots_body(capacity, routing_ref, spread_ref, first_ref, second_ref, choice_ref):
@@ -218,10 +214,8 @@
     high_12_ref,
     mine_ref,
     other_ref,
-    weight,
-    sems,
 ):
-    _, slots, depth, group = weight.shape
+    nears, slots, depth, lanes = low_ref.shape
     count = mine_ref.shape[0]
     v, u = place_ref[2], place_ref[3]
     sources = (
@@ -230,33 +224,22 @@
         (3, low_32_ref.at[0], high_3_ref),
         (2, low_32_ref.at[1], high_12_ref.at[1]),
     )
-    copies = []
-    for number, (_, *halves) in enumerate(sources):
-        for side, half in enumerate(halves):
-            for nth, near in enumerate(NEAR):
-                copy = pltpu.make_async_copy(
-                    half.at[nth],
-                    weight.at[
-                        number,
-                        pl.ds(4 * side, 4),
-                        :,
-                        pl.ds(pl.multiple_of((u ^ near) * 128, 128), 128),
-                    ],
-                    sems.at[8 * number + 4 * side + nth],
+    for far, *halves in sources:
+        weight = jnp.concatenate(
+            [
+                jnp.concatenate(
+                    [half[nth].reshape(slots * depth, lanes) for half in halves], axis=0
                 )
-                copy.start()
-                copies.append(copy)
-    for number, (far, *_) in enumerate(sources):
-        for nth in range(8):
-            copies[8 * number + nth].wait()
-        product = jnp.dot(
-            active_ref[...],
-            weight[number].reshape(slots * depth, group),
-            preferred_element_type=jnp.float32,
+                for nth in range(nears)
+            ],
+            axis=1,
         )
-        to = pl.ds(pl.multiple_of((v ^ far) * group, group), group)
-        mine_ref[:, to] = product[:count]
-        other_ref[:, to] = product[count:].astype(other_ref.dtype)
+        product = jnp.dot(active_ref[...], weight, preferred_element_type=jnp.float32)
+        for nth, near in enumerate(NEAR):
+            piece = product[:, nth * lanes : nth * lanes + lanes]
+            to = pl.ds(pl.multiple_of(((v ^ far) * nears + (u ^ near)) * lanes, lanes), lanes)
+            mine_ref[:, to] = piece[:count]
+            other_ref[:, to] = piece[count:].astype(other_ref.dtype)
 
 
 def state_body(
@@ -366,7 +349,6 @@
     z, core, y, x = tp >> 1, tp & 1, sp >> 2, sp & 3
     u, v = jnp.where(core == 0, x, y), jnp.where(core == 0, y, x)
     place = jnp.stack([z, core, v, u]).astype(jnp.int32)
-    depth = proj_weight.shape[0]
 
     gated = (
         conv_value.astype(jnp.float32) * jax.nn.sigmoid(conv_gate.astype(jnp.float32))
@@ -390,10 +372,14 @@
     high_12 = cross(jnp.stack([high, high_3]), 1, 1)
     pieces = [low, low_1, low_32, high, high_3, high_12]
 
-    convolved = convolve_tokens(place, doc_ids, gated, came, conv_kernel, 8)
+    tile = 2 * count
+    rest = convolve_tokens(4, 4, tile, doc_ids, gated, conv_kernel)
+    head = convolve_tokens(0, 4, tile, doc_ids, gated, conv_kernel, came)
+    convolved = lax.optimization_barrier(jnp.concatenate([head, rest], axis=0))
     raw = []
     for d in ORDER:
-        raw.append(swap(convolved[d], dz=d) if d else convolved[d])
+        part = lax.dynamic_index_in_dim(convolved, z ^ d, 0, keepdims=False)
+        raw.append(swap(part, dz=d) if d else part)
 
     spread, first_pick, second_pick, choice = pl.pallas_call(
         functools.partial(slots_body, capacity),
@@ -443,15 +429,11 @@
     )
     kept, given = pl.pallas_call(
         partial_body,
-        in_specs=[SMEM, VMEM] + [pl.BlockSpec(memory_space=pltpu.HBM)] * 6,
+        in_specs=[SMEM] + [VMEM] * 7,
         out_specs=[VMEM] * 2,
         out_shape=[
             jax.ShapeDtypeStruct((count, width), jnp.float32),
             jax.ShapeDtypeStruct((count, width), jnp.bfloat16),
-        ],
-        scratch_shapes=[
-            pltpu.VMEM((4, 8, depth, width // 4), jnp.bfloat16),
-            pltpu.SemaphoreType.DMA((32,)),
         ],
         compiler_params=params(24),
         name="partial",

time: 160 us -> 158 us (0.988)
  waiting for transfers between devices: 38.7 us -> 35 us
    ppermute x12, waiting for transfers between devices: 22.6 us -> 20.2 us  [swap(): lax.ppermute(array, ('sp', 'tp'), [(i, i ^ flip) for i in range(256)])]
    pallas_call x2 -> x3, Pallas kernels: 10.5 us -> 10.5 us  [the longest x2 6.81 us: convolve_tokens(): pl.pallas_call(functools.partial(conv_kernel_body, begin), in_specs=[SMEM...]
  transfers between devices with their start and end apart: 20 -> 20, of which waited for: 15 -> 12; matrix products, arithmetic and copies ran while one was open for 2% -> 2% of each run, Pallas kernels for 5% -> 6%
where the time goes in v2:
time: 158 us; the launch traced here: 155 us
  blocking collectives  57.6 us (36%)
  starting transfers between devices  39.1 us (25%)
  waiting for transfers between devices  35 us (22%)
  Pallas kernels  18.5 us (12%)
  other arithmetic  3.18 us (2%)
    all_to_all x2, blocking collectives, exchanged(): lax.all_to_all(blocks, 'sp', split_axis=0, concat_axis=0, tiled=True)  57.6 us
    ppermute x12, starting transfers between devices, swap(): lax.ppermute(array, ('sp', 'tp'), [(i, i ^ flip) for i in range(256)])  27.3 us
    ppermute x12, waiting for transfers between devices, swap(): lax.ppermute(array, ('sp', 'tp'), [(i, i ^ flip) for i in range(256)])  20.2 us
    ppermute x7, waiting for transfers between devices, cross(): return lax.ppermute(array, ('sp', 'tp'), pairs)  14.8 us
    ppermute x7, starting transfers between devices, cross(): return lax.ppermute(array, ('sp', 'tp'), pairs)  9.99 us
    pallas_call x2, Pallas kernels, convolve_tokens(): pl.pallas_call(functools.partial(conv_kernel_body, begin), in_specs=[SMEM...  6.81 us
    pallas_call x1, Pallas kernels, body(): pl.pallas_call(partial_body, in_specs=[SMEM] + [VMEM] * 7, out_specs=[VME...  3.72 us
  transfers between devices with their start and end apart: 20, of which 12 were waited for; matrix products, arithmetic and copies ran while one was open for 2% of the time, Pallas kernels for 6%

profile of v2, /device:TPU:0, one launch (start us, length us, event | category | flops | bytes accessed | tf_op | source)
XLA Modules:
  0.0 155.1 jit_solution(1391745187460411810)
XLA Ops:
  0.0 1.0 copy-done
  1.1 5.6 %collective-permute-start.9 = (bf16[1,128,128]{2,1,0:T(8,128)(2,1)S(1)}, bf16[1,128,128]{2,1,0:T(8,128)(2,1)S(1)}, u32[]{:S(2)}, u32[]{:S(2)}) collective-permute-start(bf16[1,128,128]{2,1,0:T(8,128)(2,1)S(1)} %dynamic-slice_bitcast_fusion.8), channel_id=1, source_target_pairs={{0,8},{1,9},{2,10},{3,11},{4,12},{5,13},{6,14},{7,15},{8,0},{9,1},... | collective-permute-start | bytes 98312 | tf_op jit(solution)/shard_map/ppermute | solution.py:311
  6.6 2.3 %collective-permute-done.9 = bf16[1,128,128]{2,1,0:T(8,128)(2,1)S(1)} collective-permute-done((bf16[1,128,128]{2,1,0:T(8,128)(2,1)S(1)}, bf16[1,128,128]{2,1,0:T(8,128)(2,1)S(1)}, u32[]{:S(2)}, u32[]{:S(2)}) %collective-permute-start.9) | collective-permute-done | bytes 32800 | tf_op jit(solution)/shard_map/ppermute | solution.py:311
  9.0 1.8 %collective-permute-start.10 = (bf16[2,128,128]{2,1,0:T(8,128)(2,1)S(1)}, bf16[2,128,128]{2,1,0:T(8,128)(2,1)S(1)}, u32[]{:S(2)}, u32[]{:S(2)}) collective-permute-start(bf16[2,128,128]{2,1,0:T(8,128)(2,1)S(1)} %pad_maximum_fusion.7), channel_id=1, source_target_pairs={{0,4},{1,5},{2,6},{3,7},{4,0},{5,1},{6,2},{7,3},{8,12},{9,13},{10,... | collective-permute-start | bytes 196616 | tf_op jit(solution)/shard_map/ppermute | solution.py:311
  10.7 4.2 %collective-permute-done.10 = bf16[2,128,128]{2,1,0:T(8,128)(2,1)S(1)} collective-permute-done((bf16[2,128,128]{2,1,0:T(8,128)(2,1)S(1)}, bf16[2,128,128]{2,1,0:T(8,128)(2,1)S(1)}, u32[]{:S(2)}, u32[]{:S(2)}) %collective-permute-start.10) | collective-permute-done | bytes 65568 | tf_op jit(solution)/shard_map/ppermute | solution.py:311
  15.0 0.1 collective-permute-start.11
  15.1 5.0 %collective-permute-done.11 = bf16[4,128,128]{2,1,0:T(8,128)(2,1)S(1)} collective-permute-done((bf16[4,128,128]{2,1,0:T(8,128)(2,1)S(1)}, bf16[4,128,128]{2,1,0:T(8,128)(2,1)S(1)}, u32[]{:S(2)}, u32[]{:S(2)}) %collective-permute-start.11) | collective-permute-done | bytes 131104 | tf_op jit(solution)/shard_map/ppermute | solution.py:311
  20.0 1.1 collective-permute-start.12
  21.2 2.1 %collective-permute-start.13 = (bf16[8,128,128]{2,1,0:T(8,128)(2,1)S(1)}, bf16[8,128,128]{2,1,0:T(8,128)(2,1)S(1)}, u32[]{:S(2)}, u32[]{:S(2)}) collective-permute-start(bf16[8,128,128]{2,1,0:T(8,128)(2,1)S(1)} %pad_maximum_fusion.5), channel_id=1, source_target_pairs={{0,48},{1,193},{2,50},{3,195},{4,52},{5,197},{6,54},{7,199},{8,56}... | collective-permute-start | bytes 786440 | tf_op jit(solution)/shard_map/ppermute | solution.py:316
  23.3 1.0 collective-permute-start.14
  24.2 2.3 %collective-permute-done.12 = bf16[8,128,128]{2,1,0:T(8,128)(2,1)S(1)} collective-permute-done((bf16[8,128,128]{2,1,0:T(8,128)(2,1)S(1)}, bf16[8,128,128]{2,1,0:T(8,128)(2,1)S(1)}, u32[]{:S(2)}, u32[]{:S(2)}) %collective-permute-start.12) | collective-permute-done | bytes 262176 | tf_op jit(solution)/shard_map/ppermute | solution.py:316
  26.5 5.4 %collective-permute-done.13 = bf16[8,128,128]{2,1,0:T(8,128)(2,1)S(1)} collective-permute-done((bf16[8,128,128]{2,1,0:T(8,128)(2,1)S(1)}, bf16[8,128,128]{2,1,0:T(8,128)(2,1)S(1)}, u32[]{:S(2)}, u32[]{:S(2)}) %collective-permute-start.13) | collective-permute-done | bytes 262176 | tf_op jit(solution)/shard_map/ppermute | solution.py:316
  32.0 0.1 fusion.1
  32.1 3.1 %collective-permute-start.17 = (bf16[4,4,128,128]{3,2,1,0:T(8,128)(2,1)S(1)}, bf16[4,4,128,128]{3,2,1,0:T(8,128)(2,1)S(1)}, u32[]{:S(2)}, u32[]{:S(2)}) collective-permute-start(bf16[4,4,128,128]{3,2,1,0:T(8,128)(2,1)S(1)} %get-tuple-element.32.high_ref), channel_id=1, source_target_pairs={{0,192},{1,49},{2,194},{3,51},{4,196},{5,53},{6,198},{7,55},{8,200... | collective-permute-start | bytes 1572872 | tf_op jit(solution)/shard_map/ppermute | solution.py:316
  35.2 0.1 fusion.2
  35.3 0.2 collective-permute-start.15
  35.5 0.4 multiply_convert_fusion.gated_ref
  35.9 6.6 %collective-permute-done.17.high_3_ref = bf16[4,4,128,128]{3,2,1,0:T(8,128)(2,1)S(1)} collective-permute-done((bf16[4,4,128,128]{3,2,1,0:T(8,128)(2,1)S(1)}, bf16[4,4,128,128]{3,2,1,0:T(8,128)(2,1)S(1)}, u32[]{:S(2)}, u32[]{:S(2)}) %collective-permute-start.17) | collective-permute-done | bytes 524320 | tf_op jit(solution)/shard_map/ppermute | solution.py:316
  42.5 1.1 pad_maximum_fusion.1
  43.6 0.4 collective-permute-start.18
  44.0 0.5 collective-permute-done.15.low_1_ref
  44.5 1.1 pad_maximum_fusion
  45.6 2.1 %collective-permute-start.16 = (bf16[2,4,4,128,128]{4,3,2,1,0:T(8,128)(2,1)}, bf16[2,4,4,128,128]{4,3,2,1,0:T(8,128)(2,1)}, u32[]{:S(2)}, u32[]{:S(2)}) collective-permute-start(bf16[2,4,4,128,128]{4,3,2,1,0:T(8,128)(2,1)} %pad_maximum_fusion), channel_id=1, source_target_pairs={{0,192},{1,49},{2,194},{3,51},{4,196},{5,53},{6,198},{7,55},{8,200... | collective-permute-start | bytes 3145736 | tf_op jit(solution)/shard_map/ppermute | solution.py:316
  48.0 1.8 %collective-permute-start = (bf16[64,128]{1,0:T(8,128)(2,1)S(1)}, bf16[64,128]{1,0:T(8,128)(2,1)S(1)}, u32[]{:S(2)}, u32[]{:S(2)}) collective-permute-start(bf16[64,128]{1,0:T(8,128)(2,1)S(1)} %pad_maximum_fusion.8), channel_id=1, source_target_pairs={{0,16},{16,32},{32,48},{48,64},{64,80},{80,96},{96,112},{112,128},... | collective-permute-start | bytes 49160 | tf_op jit(solution)/shard_map/ppermute | solution.py:322
  49.8 3.5 %conv_rest.1 = bf16[4,384,128]{2,1,0:T(8,128)(2,1)S(1)} custom-call(s32[3072]{0:T(1024)S(1)} %copy-done.5, s32[24,128]{1,0:T(8,128)S(1)} %bitcast.66, bf16[3072,128]{1,0:T(8,128)(2,1)S(1)} %multiply_convert_fusion.gated_ref, bf16[31,128]{1,0:T(8,128)(2,1)S(1)} %copy-done.6), custom_call_target="tpu_custom_call" | custom-call | tf_op jit(solution)/shard_map/conv_rest/pallas_call | solution.py:111
  53.3 3.3 %conv_head.1 = bf16[4,384,128]{2,1,0:T(8,128)(2,1)S(1)} custom-call(s32[3072]{0:T(1024)S(1)} %copy-done.5, s32[24,128]{1,0:T(8,128)S(1)} %bitcast.67, bf16[3072,128]{1,0:T(8,128)(2,1)S(1)} %multiply_convert_fusion.gated_ref, bf16[31,128]{1,0:T(8,128)(2,1)S(1)} %copy-done.6, bf16[64,128]{1,0:T(8,128)(2,1)S(1)} %collective-permute-done.refs_0_), custom_call_target="tpu_custom_call" | custom-call | tf_op jit(solution)/shard_map/conv_head/pallas_call | solution.py:111
  56.9 5.3 %collective-permute-start.1 = (bf16[384,128]{1,0:T(8,128)(2,1)S(1)}, bf16[384,128]{1,0:T(8,128)(2,1)S(1)}, u32[]{:S(2)}, u32[]{:S(2)}) collective-permute-start(bf16[384,128]{1,0:T(8,128)(2,1)S(1)} %get-tuple-element.29), channel_id=1, source_target_pairs={{0,8},{1,9},{2,10},{3,11},{4,12},{5,13},{6,14},{7,15},{8,0},{9,1},... | collective-permute-start | bytes 294920 | tf_op jit(solution)/shard_map/ppermute | solution.py:311
  62.1 2.0 %collective-permute-start.2 = (bf16[384,128]{1,0:T(8,128)(2,1)S(1)}, bf16[384,128]{1,0:T(8,128)(2,1)S(1)}, u32[]{:S(2)}, u32[]{:S(2)}) collective-permute-start(bf16[384,128]{1,0:T(8,128)(2,1)S(1)} %get-tuple-element.28), channel_id=1, source_target_pairs={{0,4},{1,5},{2,6},{3,7},{4,0},{5,1},{6,2},{7,3},{8,12},{9,13},{10,... | collective-permute-start | bytes 294920 | tf_op jit(solution)/shard_map/ppermute | solution.py:311
  64.1 2.6 %collective-permute-done.1.refs_1_ = bf16[384,128]{1,0:T(8,128)(2,1)S(1)} collective-permute-done((bf16[384,128]{1,0:T(8,128)(2,1)S(1)}, bf16[384,128]{1,0:T(8,128)(2,1)S(1)}, u32[]{:S(2)}, u32[]{:S(2)}) %collective-permute-start.1) | collective-permute-done | bytes 98336 | tf_op jit(solution)/shard_map/ppermute | solution.py:311
  66.7 2.8 %collective-permute-start.4 = (bf16[384,128]{1,0:T(8,128)(2,1)S(1)}, bf16[384,128]{1,0:T(8,128)(2,1)S(1)}, u32[]{:S(2)}, u32[]{:S(2)}) collective-permute-start(bf16[384,128]{1,0:T(8,128)(2,1)S(1)} %get-tuple-element.26), channel_id=1, source_target_pairs={{0,2},{1,3},{2,0},{3,1},{4,6},{5,7},{6,4},{7,5},{8,10},{9,11},{10,... | collective-permute-start | bytes 294920 | tf_op jit(solution)/shard_map/ppermute | solution.py:311
  69.5 5.0 %collective-permute-start.5 = (bf16[384,128]{1,0:T(8,128)(2,1)S(1)}, bf16[384,128]{1,0:T(8,128)(2,1)S(1)}, u32[]{:S(2)}, u32[]{:S(2)}) collective-permute-start(bf16[384,128]{1,0:T(8,128)(2,1)S(1)} %get-tuple-element.25), channel_id=1, source_target_pairs={{0,10},{1,11},{2,8},{3,9},{4,14},{5,15},{6,12},{7,13},{8,2},{9,3},... | collective-permute-start | bytes 294920 | tf_op jit(solution)/shard_map/ppermute | solution.py:311
  74.5 1.1 collective-permute-start.6
  75.6 3.4 %collective-permute-start.7 = (bf16[384,128]{1,0:T(8,128)(2,1)S(1)}, bf16[384,128]{1,0:T(8,128)(2,1)S(1)}, u32[]{:S(2)}, u32[]{:S(2)}) collective-permute-start(bf16[384,128]{1,0:T(8,128)(2,1)S(1)} %get-tuple-element.23), channel_id=1, source_target_pairs={{0,14},{1,15},{2,12},{3,13},{4,10},{5,11},{6,8},{7,9},{8,6},{9,7},... | collective-permute-start | bytes 294920 | tf_op jit(solution)/shard_map/ppermute | solution.py:311
  79.0 2.2 %collective-permute-done.6.refs_6_ = bf16[384,128]{1,0:T(8,128)(2,1)S(1)} collective-permute-done((bf16[384,128]{1,0:T(8,128)(2,1)S(1)}, bf16[384,128]{1,0:T(8,128)(2,1)S(1)}, u32[]{:S(2)}, u32[]{:S(2)}) %collective-permute-start.6) | collective-permute-done | bytes 98336 | tf_op jit(solution)/shard_map/ppermute | solution.py:311
  81.2 1.0 collective-permute-done.7.refs_7_
  82.2 0.4 stats.1.mine_ref
  82.8 1.3 collective-permute-done.8.other_ref
  84.2 1.2 activate.1.active_ref
  85.4 3.7 %partial.1 = (f32[192,2048]{1,0:T(8,128)S(1)}, bf16[192,2048]{1,0:T(8,128)(2,1)S(1)}) custom-call(s32[4]{0:T(128)S(1)} %pad_add_fusion.place_ref, bf16[384,1024]{1,0:T(8,128)(2,1)S(1)} %activate.1.active_ref, bf16[4,4,128,128]{3,2,1,0:T(8,128)(2,1)S(1)} %get-tuple-element.34.low_ref, bf16[4,4,128,128]{3,2,1,0:T(8,128)(2,1)S(1)} %collective-permute-done.15.low_1_ref, ...), custom_call_target="tpu_custom_call" | custom-call | tf_op jit(solution)/shard_map/partial/pallas_call | solution.py:430
  89.1 0.2 collective-permute-start.19
  89.4 0.4 slots.1
  89.9 0.1 maximum_maximum_fusion.router_ref
  89.9 1.6 %collective-permute-done.19.other_ref = bf16[192,2048]{1,0:T(8,128)(2,1)S(1)} collective-permute-done((bf16[192,2048]{1,0:T(8,128)(2,1)S(1)}, bf16[192,2048]{1,0:T(8,128)(2,1)S(1)}, u32[]{:S(2)}, u32[]{:S(2)}) %collective-permute-start.19) | collective-permute-done | bytes 786464 | tf_op jit(solution)/shard_map/ppermute | solution.py:311
  91.5 1.4 state.1
  92.9 32.4 %all_to_all.10 = bf16[16,24,2048]{2,1,0:T(8,128)(2,1)S(1)} all-to-all(bf16[16,24,2048]{2,1,0:T(8,128)(2,1)S(1)} %bitcast.65), channel_id=1, replica_groups=mesh['sp'=16,'tp'=16] {'sp'}, dimensions={0} | all-to-all | bytes 3145728 | tf_op jit(solution)/shard_map/all_to_all | solution.py:464
  125.3 2.6 %experts.1 = bf16[384,2048]{1,0:T(8,128)(2,1)S(1)} custom-call(bf16[384,2048]{1,0:T(8,128)(2,1)S(1)} %bitcast.58, bf16[2048,512]{1,0:T(8,128)(2,1)S(1)} %bitcast.62, bf16[2048,512]{1,0:T(8,128)(2,1)S(1)} %bitcast.63, bf16[512,2048]{1,0:T(8,128)(2,1)S(1)} %bitcast.64), custom_call_target="tpu_custom_call" | custom-call | tf_op jit(solution)/shard_map/experts/pallas_call | solution.py:468
  128.0 25.2 %all_to_all.11 = bf16[16,24,2048]{2,1,0:T(8,128)(2,1)S(1)} all-to-all(bf16[16,24,2048]{2,1,0:T(8,128)(2,1)S(1)} %bitcast.59), channel_id=1, replica_groups=mesh['sp'=16,'tp'=16] {'sp'}, dimensions={0} | all-to-all | bytes 3145728 | tf_op jit(solution)/shard_map/all_to_all | solution.py:464
  153.2 2.0 %mix.1 = bf16[192,2048]{1,0:T(8,128)(2,1)} custom-call(bf16[192,2048]{1,0:T(8,128)(2,1)S(1)} %get-tuple-element.18.state_ref, bf16[192,384]{1,0:T(8,128)(2,1)S(1)} %get-tuple-element.19.first_ref, bf16[192,384]{1,0:T(8,128)(2,1)S(1)} %get-tuple-element.20.second_ref, f32[192,32]{1,0:T(8,128)S(1)} %get-tuple-element.21.mix_ref, bf16[384,2048]{1,0:T(8,128)(2,1)S(1)} %bitcast.57), custom_call_target="tpu_custom_call" | custom-call | tf_op jit(solution)/shard_map/mix/pallas_call | solution.py:476
  (55 shorter events, 0.8 us)
Async XLA Ops:
  0.0 1.0 copy-start
  1.1 7.9 %collective-permute-start.9 = (bf16[1,128,128]{2,1,0:T(8,128)(2,1)S(1)}, bf16[1,128,128]{2,1,0:T(8,128)(2,1)S(1)}, u32[]{:S(2)}, u32[]{:S(2)}) collective-permute-start(bf16[1,128,128]{2,1,0:T(8,128)(2,1)S(1)} %dynamic-slice_bitcast_fusion.8), channel_id=1, source_target_pairs={{0,8},{1,9},{2,10},{3,11},{4,12},{5,13},{6,14},{7,15},{8,0},{9,1},... | collective-permute-start | bytes 98312 | tf_op jit(solution)/shard_map/ppermute | solution.py:311
  9.0 6.0 %collective-permute-start.10 = (bf16[2,128,128]{2,1,0:T(8,128)(2,1)S(1)}, bf16[2,128,128]{2,1,0:T(8,128)(2,1)S(1)}, u32[]{:S(2)}, u32[]{:S(2)}) collective-permute-start(bf16[2,128,128]{2,1,0:T(8,128)(2,1)S(1)} %pad_maximum_fusion.7), channel_id=1, source_target_pairs={{0,4},{1,5},{2,6},{3,7},{4,0},{5,1},{6,2},{7,3},{8,12},{9,13},{10,... | collective-permute-start | bytes 196616 | tf_op jit(solution)/shard_map/ppermute | solution.py:311
  15.0 5.1 %collective-permute-start.11 = (bf16[4,128,128]{2,1,0:T(8,128)(2,1)S(1)}, bf16[4,128,128]{2,1,0:T(8,128)(2,1)S(1)}, u32[]{:S(2)}, u32[]{:S(2)}) collective-permute-start(bf16[4,128,128]{2,1,0:T(8,128)(2,1)S(1)} %get-tuple-element.42), channel_id=1, source_target_pairs={{0,2},{1,3},{2,0},{3,1},{4,6},{5,7},{6,4},{7,5},{8,10},{9,11},{10,... | collective-permute-start | bytes 393224 | tf_op jit(solution)/shard_map/ppermute | solution.py:311
  20.0 6.5 %collective-permute-start.12 = (bf16[8,128,128]{2,1,0:T(8,128)(2,1)S(1)}, bf16[8,128,128]{2,1,0:T(8,128)(2,1)S(1)}, u32[]{:S(2)}, u32[]{:S(2)}) collective-permute-start(bf16[8,128,128]{2,1,0:T(8,128)(2,1)S(1)} %pad_maximum_fusion.5), channel_id=1, source_target_pairs={{0,16},{1,65},{2,18},{3,67},{4,20},{5,69},{6,22},{7,71},{8,24},{9,... | collective-permute-start | bytes 786440 | tf_op jit(solution)/shard_map/ppermute | solution.py:316
  21.2 10.7 %collective-permute-start.13 = (bf16[8,128,128]{2,1,0:T(8,128)(2,1)S(1)}, bf16[8,128,128]{2,1,0:T(8,128)(2,1)S(1)}, u32[]{:S(2)}, u32[]{:S(2)}) collective-permute-start(bf16[8,128,128]{2,1,0:T(8,128)(2,1)S(1)} %pad_maximum_fusion.5), channel_id=1, source_target_pairs={{0,48},{1,193},{2,50},{3,195},{4,52},{5,197},{6,54},{7,199},{8,56}... | collective-permute-start | bytes 786440 | tf_op jit(solution)/shard_map/ppermute | solution.py:316
  23.3 8.6 %collective-permute-start.14 = (bf16[8,128,128]{2,1,0:T(8,128)(2,1)S(1)}, bf16[8,128,128]{2,1,0:T(8,128)(2,1)S(1)}, u32[]{:S(2)}, u32[]{:S(2)}) collective-permute-start(bf16[8,128,128]{2,1,0:T(8,128)(2,1)S(1)} %pad_maximum_fusion.5), channel_id=1, source_target_pairs={{0,32},{1,129},{2,34},{3,131},{4,36},{5,133},{6,38},{7,135},{8,40}... | collective-permute-start | bytes 786440 | tf_op jit(solution)/shard_map/ppermute | solution.py:316
  31.9 3.5 %copy-start.11 = (bf16[3072,128]{1,0:T(8,128)(2,1)S(1)}, bf16[3072,128]{1,0:T(8,128)(2,1)}, u32[]{:S(2)}) copy-start(bf16[3072,128]{1,0:T(8,128)(2,1)} %param.16) | copy-start | bytes 2359300
  32.0 3.5 %copy-start.12 = (bf16[3072,128]{1,0:T(8,128)(2,1)S(1)}, bf16[3072,128]{1,0:T(8,128)(2,1)}, u32[]{:S(2)}) copy-start(bf16[3072,128]{1,0:T(8,128)(2,1)} %param.15) | copy-start | bytes 2359300
  32.1 10.5 %collective-permute-start.17 = (bf16[4,4,128,128]{3,2,1,0:T(8,128)(2,1)S(1)}, bf16[4,4,128,128]{3,2,1,0:T(8,128)(2,1)S(1)}, u32[]{:S(2)}, u32[]{:S(2)}) collective-permute-start(bf16[4,4,128,128]{3,2,1,0:T(8,128)(2,1)S(1)} %get-tuple-element.32.high_ref), channel_id=1, source_target_pairs={{0,192},{1,49},{2,194},{3,51},{4,196},{5,53},{6,198},{7,55},{8,200... | collective-permute-start | bytes 1572872 | tf_op jit(solution)/shard_map/ppermute | solution.py:316
  35.3 9.3 %collective-permute-start.15 = (bf16[4,4,128,128]{3,2,1,0:T(8,128)(2,1)S(1)}, bf16[4,4,128,128]{3,2,1,0:T(8,128)(2,1)S(1)}, u32[]{:S(2)}, u32[]{:S(2)}) collective-permute-start(bf16[4,4,128,128]{3,2,1,0:T(8,128)(2,1)S(1)} %get-tuple-element.34.low_ref), channel_id=1, source_target_pairs={{0,64},{1,17},{2,66},{3,19},{4,68},{5,21},{6,70},{7,23},{8,72},{9,... | collective-permute-start | bytes 1572872 | tf_op jit(solution)/shard_map/ppermute | solution.py:316
  43.6 4.1 %copy-start.5 = (s32[3072]{0:T(1024)S(1)}, s32[3072]{0:T(1024)}, u32[]{:S(2)}) copy-start(s32[3072]{0:T(1024)} %ids_ref.3) | copy-start | bytes 36868
  43.6 6.2 %copy-start.6 = (bf16[31,128]{1,0:T(8,128)(2,1)S(1)}, bf16[31,128]{1,0:T(8,128)(2,1)}, u32[]{:S(2)}) copy-start(bf16[31,128]{1,0:T(8,128)(2,1)} %kernel_ref.3) | copy-start | bytes 23812
  43.6 41.8 %collective-permute-start.18 = (bf16[2,4,4,128,128]{4,3,2,1,0:T(8,128)(2,1)}, bf16[2,4,4,128,128]{4,3,2,1,0:T(8,128)(2,1)}, u32[]{:S(2)}, u32[]{:S(2)}) collective-permute-start(bf16[2,4,4,128,128]{4,3,2,1,0:T(8,128)(2,1)} %pad_maximum_fusion.1), channel_id=1, source_target_pairs={{0,64},{1,17},{2,66},{3,19},{4,68},{5,21},{6,70},{7,23},{8,72},{9,... | collective-permute-start | bytes 3145736 | tf_op jit(solution)/shard_map/ppermute | solution.py:316
  45.6 39.8 %collective-permute-start.16 = (bf16[2,4,4,128,128]{4,3,2,1,0:T(8,128)(2,1)}, bf16[2,4,4,128,128]{4,3,2,1,0:T(8,128)(2,1)}, u32[]{:S(2)}, u32[]{:S(2)}) collective-permute-start(bf16[2,4,4,128,128]{4,3,2,1,0:T(8,128)(2,1)} %pad_maximum_fusion), channel_id=1, source_target_pairs={{0,192},{1,49},{2,194},{3,51},{4,196},{5,53},{6,198},{7,55},{8,200... | collective-permute-start | bytes 3145736 | tf_op jit(solution)/shard_map/ppermute | solution.py:316
  48.0 5.3 %collective-permute-start = (bf16[64,128]{1,0:T(8,128)(2,1)S(1)}, bf16[64,128]{1,0:T(8,128)(2,1)S(1)}, u32[]{:S(2)}, u32[]{:S(2)}) collective-permute-start(bf16[64,128]{1,0:T(8,128)(2,1)S(1)} %pad_maximum_fusion.8), channel_id=1, source_target_pairs={{0,16},{16,32},{32,48},{48,64},{64,80},{80,96},{96,112},{112,128},... | collective-permute-start | bytes 49160 | tf_op jit(solution)/shard_map/ppermute | solution.py:322
  56.7 27.4 %copy-start.7 = (f32[2048]{0:T(1024)S(1)}, f32[2048]{0:T(1024)}, u32[]{:S(2)}) copy-start(f32[2048]{0:T(1024)} %param.19) | copy-start | bytes 24580
  56.8 27.4 %copy-start.8 = (f32[2048]{0:T(1024)S(1)}, f32[2048]{0:T(1024)}, u32[]{:S(2)}) copy-start(f32[2048]{0:T(1024)} %param.20) | copy-start | bytes 24580
  56.9 9.8 %collective-permute-start.1 = (bf16[384,128]{1,0:T(8,128)(2,1)S(1)}, bf16[384,128]{1,0:T(8,128)(2,1)S(1)}, u32[]{:S(2)}, u32[]{:S(2)}) collective-permute-start(bf16[384,128]{1,0:T(8,128)(2,1)S(1)} %get-tuple-element.29), channel_id=1, source_target_pairs={{0,8},{1,9},{2,10},{3,11},{4,12},{5,13},{6,14},{7,15},{8,0},{9,1},... | collective-permute-start | bytes 294920 | tf_op jit(solution)/shard_map/ppermute | solution.py:311
  62.1 7.3 %collective-permute-start.2 = (bf16[384,128]{1,0:T(8,128)(2,1)S(1)}, bf16[384,128]{1,0:T(8,128)(2,1)S(1)}, u32[]{:S(2)}, u32[]{:S(2)}) collective-permute-start(bf16[384,128]{1,0:T(8,128)(2,1)S(1)} %get-tuple-element.28), channel_id=1, source_target_pairs={{0,4},{1,5},{2,6},{3,7},{4,0},{5,1},{6,2},{7,3},{8,12},{9,13},{10,... | collective-permute-start | bytes 294920 | tf_op jit(solution)/shard_map/ppermute | solution.py:311
  64.1 10.3 %collective-permute-start.3 = (bf16[384,128]{1,0:T(8,128)(2,1)S(1)}, bf16[384,128]{1,0:T(8,128)(2,1)S(1)}, u32[]{:S(2)}, u32[]{:S(2)}) collective-permute-start(bf16[384,128]{1,0:T(8,128)(2,1)S(1)} %get-tuple-element.27), channel_id=1, source_target_pairs={{0,12},{1,13},{2,14},{3,15},{4,8},{5,9},{6,10},{7,11},{8,4},{9,5},... | collective-permute-start | bytes 294920 | tf_op jit(solution)/shard_map/ppermute | solution.py:311
  66.7 8.9 %collective-permute-start.4 = (bf16[384,128]{1,0:T(8,128)(2,1)S(1)}, bf16[384,128]{1,0:T(8,128)(2,1)S(1)}, u32[]{:S(2)}, u32[]{:S(2)}) collective-permute-start(bf16[384,128]{1,0:T(8,128)(2,1)S(1)} %get-tuple-element.26), channel_id=1, source_target_pairs={{0,2},{1,3},{2,0},{3,1},{4,6},{5,7},{6,4},{7,5},{8,10},{9,11},{10,... | collective-permute-start | bytes 294920 | tf_op jit(solution)/shard_map/ppermute | solution.py:311
  69.5 9.5 %collective-permute-start.5 = (bf16[384,128]{1,0:T(8,128)(2,1)S(1)}, bf16[384,128]{1,0:T(8,128)(2,1)S(1)}, u32[]{:S(2)}, u32[]{:S(2)}) collective-permute-start(bf16[384,128]{1,0:T(8,128)(2,1)S(1)} %get-tuple-element.25), channel_id=1, source_target_pairs={{0,10},{1,11},{2,8},{3,9},{4,14},{5,15},{6,12},{7,13},{8,2},{9,3},... | collective-permute-start | bytes 294920 | tf_op jit(solution)/shard_map/ppermute | solution.py:311
  74.5 6.7 %collective-permute-start.6 = (bf16[384,128]{1,0:T(8,128)(2,1)S(1)}, bf16[384,128]{1,0:T(8,128)(2,1)S(1)}, u32[]{:S(2)}, u32[]{:S(2)}) collective-permute-start(bf16[384,128]{1,0:T(8,128)(2,1)S(1)} %get-tuple-element.24), channel_id=1, source_target_pairs={{0,6},{1,7},{2,4},{3,5},{4,2},{5,3},{6,0},{7,1},{8,14},{9,15},{10,... | collective-permute-start | bytes 294920 | tf_op jit(solution)/shard_map/ppermute | solution.py:311
  75.6 6.6 %collective-permute-start.7 = (bf16[384,128]{1,0:T(8,128)(2,1)S(1)}, bf16[384,128]{1,0:T(8,128)(2,1)S(1)}, u32[]{:S(2)}, u32[]{:S(2)}) collective-permute-start(bf16[384,128]{1,0:T(8,128)(2,1)S(1)} %get-tuple-element.23), channel_id=1, source_target_pairs={{0,14},{1,15},{2,12},{3,13},{4,10},{5,11},{6,8},{7,9},{8,6},{9,7},... | collective-permute-start | bytes 294920 | tf_op jit(solution)/shard_map/ppermute | solution.py:311
  82.6 1.5 collective-permute-start.8
  85.3 4.0 %copy-start.10 = (s32[192,2]{0,1:T(2,128)S(1)}, s32[192,2]{0,1:T(2,128)}, u32[]{:S(2)}) copy-start(s32[192,2]{0,1:T(2,128)} %param.26) | copy-start | bytes 4612
  85.3 4.5 %copy-start.13 = (bf16[2048,16]{0,1:T(8,128)(2,1)S(1)}, bf16[2048,16]{0,1:T(8,128)(2,1)}, u32[]{:S(2)}) copy-start(bf16[2048,16]{0,1:T(8,128)(2,1)} %param.25) | copy-start | bytes 196612
  85.3 4.5 %copy-start.14 = (bf16[2048,2]{0,1:T(2,128)(2,1)S(1)}, bf16[2048,2]{0,1:T(2,128)(2,1)}, u32[]{:S(2)}) copy-start(bf16[2048,2]{0,1:T(2,128)(2,1)} %param.24) | copy-start | bytes 24580
  85.4 6.1 %copy-start.4 = (bf16[192,2048]{1,0:T(8,128)(2,1)S(1)}, bf16[192,2048]{1,0:T(8,128)(2,1)}, u32[]{:S(2)}) copy-start(bf16[192,2048]{1,0:T(8,128)(2,1)} %residual_ref.1) | copy-start | bytes 2359300
  85.4 6.1 %copy-start.9 = (f32[2048]{0:T(1024)S(1)}, f32[2048]{0:T(1024)}, u32[]{:S(2)}) copy-start(f32[2048]{0:T(1024)} %param.23) | copy-start | bytes 24580
  89.1 2.4 %collective-permute-start.19 = (bf16[192,2048]{1,0:T(8,128)(2,1)S(1)}, bf16[192,2048]{1,0:T(8,128)(2,1)S(1)}, u32[]{:S(2)}, u32[]{:S(2)}) collective-permute-start(bf16[192,2048]{1,0:T(8,128)(2,1)S(1)} %get-tuple-element.15), channel_id=1, source_target_pairs={{0,1},{1,0},{2,3},{3,2},{4,5},{5,4},{6,7},{7,6},{8,9},{9,8},{10,11... | collective-permute-start | bytes 2359304 | tf_op jit(solution)/shard_map/ppermute | solution.py:311
  91.5 33.8 %copy-start.2 = (bf16[1,2048,512]{2,1,0:T(8,128)(2,1)S(1)}, bf16[1,2048,512]{2,1,0:T(8,128)(2,1)}, u32[]{:S(2)}) copy-start(bf16[1,2048,512]{2,1,0:T(8,128)(2,1)} %param.28) | copy-start | bytes 6291460
  91.5 33.8 %copy-start.3 = (bf16[1,512,2048]{2,1,0:T(8,128)(2,1)S(1)}, bf16[1,512,2048]{2,1,0:T(8,128)(2,1)}, u32[]{:S(2)}) copy-start(bf16[1,512,2048]{2,1,0:T(8,128)(2,1)} %param.29) | copy-start | bytes 6291460
  92.9 32.4 %copy-start.1 = (bf16[1,2048,512]{2,1,0:T(8,128)(2,1)S(1)}, bf16[1,2048,512]{2,1,0:T(8,128)(2,1)}, u32[]{:S(2)}) copy-start(bf16[1,2048,512]{2,1,0:T(8,128)(2,1)} %param.27) | copy-start | bytes 6291460
